TPU v7x, 512 devices: a whole 4x4x16 slice. The times are simulated.
512 devices in a mesh: sp: 16 (over z), dp: 32 (over y, x, core).
Axes of the slice: x: 4, y: 4, z: 16, core: 2. Of those that a mesh axis runs over, the one named last changes fastest.
Arguments:
- tokens: bfloat16 [32, 3072, 2048], P('dp', 'sp'), may hold values from -36 to 36
- query_weight: bfloat16 [2048, 2048], P('dp'), may hold values from -0.125 to 0.125
- key_weight: bfloat16 [2048, 512], P('dp'), may hold values from -0.125 to 0.125
- value_weight: bfloat16 [2048, 512], P('dp'), may hold values from -0.125 to 0.125
- forget_weight: bfloat16 [2048, 16], replicated, may hold values from -0.125 to 0.125
- forget_bias: float32 [16], replicated, may hold values from 3.4 to 9
Outputs:
- mixed: bfloat16 [32, 3072, 2048], P('dp', 'sp')
All inputs are finite; a program needn't handle non-finite values.
Results may differ from a plain program's by a relative error of at most 0.012.
Values may be sent and summed in bfloat16 or wider, within the bound.
A program may use at most 64 MiB of HBM per device.

v0:
```python
import jax
import jax.numpy as jnp
from jax import lax
from jax.sharding import PartitionSpec as P


def in_one_piece(arrays, axis, dim, along):
    ends, at = ([], 0)
    for a in arrays[:-1]:
        at += a.shape[along]
        ends.append(at)
    both = jnp.concatenate(arrays, axis=along)
    return tuple(jnp.split(lax.all_gather(both, axis, axis=dim, tiled=True), ends, axis=along))


def pick_block(length):
    for candidate in (512, 384, 256, 128):
        return candidate
    return length


def on_device(tokens, query_weight, key_weight, value_weight, forget_weight, forget_bias):
    token_rows = tokens[0]
    row_count = token_rows.shape[0]
    sp_count = lax.axis_size("sp")
    head_count = forget_weight.shape[1]
    query_width = query_weight.shape[1]
    key_width = key_weight.shape[1]
    head_dim = query_width // head_count
    key_heads = key_width // head_dim
    pieces = in_one_piece((query_weight, key_weight, value_weight), "dp", 0, 1)
    query_rows, key_rows, value_rows = tuple(
        (
            jnp.dot(token_rows, weight_piece, preferred_element_type=jnp.float32)
            for weight_piece in pieces
        )
    )
    query_rows = query_rows.astype(jnp.bfloat16)
    key_rows = key_rows.astype(jnp.bfloat16)
    value_rows = value_rows.astype(jnp.bfloat16)
    gate_input = (
        jnp.dot(token_rows, forget_weight, preferred_element_type=jnp.float32)
        + forget_bias[None, :]
    )
    log_gate = jax.nn.log_sigmoid(gate_input).astype(jnp.bfloat16)
    repeats = max(1, sp_count // key_heads)
    key_rows = jnp.repeat(key_rows.reshape(row_count, key_heads, head_dim), repeats, axis=1)
    key_rows = key_rows.reshape(row_count, key_heads * repeats * head_dim)
    value_rows = jnp.repeat(value_rows.reshape(row_count, key_heads, head_dim), repeats, axis=1)
    value_rows = value_rows.reshape(row_count, key_heads * repeats * head_dim)
    head_query, head_keys, head_values, head_gates = (
        lax.all_to_all(query_rows, "sp", split_axis=1, concat_axis=0, tiled=True),
        lax.all_to_all(key_rows, "sp", split_axis=1, concat_axis=0, tiled=True),
        lax.all_to_all(value_rows, "sp", split_axis=1, concat_axis=0, tiled=True),
        lax.all_to_all(log_gate, "sp", split_axis=1, concat_axis=0, tiled=True),
    )
    seq_length = head_query.shape[0]
    local_heads = head_count // sp_count
    local_keys = head_keys.shape[1] // head_dim
    group_share = local_heads // local_keys
    decay_sum = jnp.cumsum(head_gates.astype(jnp.float32), axis=0)
    decay_grid = decay_sum.T.reshape(local_keys, group_share, seq_length)
    grouped = head_query.reshape(seq_length, local_keys, group_share, head_dim)
    key_grid = head_keys.reshape(seq_length, local_keys, head_dim)
    value_grid = head_values.reshape(seq_length, local_keys, head_dim)
    block_size = pick_block(seq_length)
    block_count = seq_length // block_size
    score_scale = head_dim ** (-0.5)
    offsets = jnp.arange(block_size, dtype=jnp.int32)

    def query_block(block_index):
        first_row = block_index * block_size
        query_part = lax.dynamic_slice_in_dim(grouped, first_row, block_size, 0)
        query_decay = lax.dynamic_slice_in_dim(decay_grid, first_row, block_size, 2)

        def fill_scores(key_block, buffer):
            key_first = key_block * block_size
            key_part = lax.dynamic_slice_in_dim(key_grid, key_first, block_size, 0)
            key_decay = lax.dynamic_slice_in_dim(decay_grid, key_first, block_size, 2)
            raw_scores = jnp.einsum(
                "qkgd,skd->kgqs", query_part, key_part, preferred_element_type=jnp.float32
            )
            biased = raw_scores * score_scale + query_decay[..., :, None] - key_decay[..., None, :]
            allowed = (key_first + offsets)[None, :] <= (first_row + offsets)[:, None]
            masked = jnp.where(allowed, biased, -jnp.inf)
            return lax.dynamic_update_index_in_dim(buffer, masked, key_block, 0)

        score_buffer = lax.fori_loop(
            0,
            block_index + 1,
            fill_scores,
            jnp.full(
                (block_count, local_keys, group_share, block_size, block_size),
                -jnp.inf,
                jnp.float32,
            ),
        )
        row_max = jnp.max(jnp.max(score_buffer, axis=-1), axis=0)
        row_sum = jnp.sum(
            jnp.sum(jnp.exp(score_buffer - row_max[None, ..., None]), axis=-1), axis=0
        )

        def weighted(key_block, accumulated):
            block_scores = lax.dynamic_index_in_dim(score_buffer, key_block, 0, keepdims=False)
            weights = (jnp.exp(block_scores - row_max[..., None]) / row_sum[..., None]).astype(
                jnp.bfloat16
            )
            value_part = lax.dynamic_slice_in_dim(value_grid, key_block * block_size, block_size, 0)
            return accumulated + jnp.einsum(
                "kgqs,skd->qkgd", weights, value_part, preferred_element_type=jnp.float32
            )

        mixed_block = lax.fori_loop(
            0,
            block_index + 1,
            weighted,
            jnp.zeros((block_size, local_keys, group_share, head_dim), jnp.float32),
        )
        return mixed_block.astype(jnp.bfloat16).reshape(block_size, local_heads * head_dim)

    head_mixed = lax.map(query_block, jnp.arange(block_count, dtype=jnp.int32))
    head_mixed = head_mixed.reshape(seq_length, local_heads * head_dim)
    mixed = lax.all_to_all(head_mixed, "sp", split_axis=0, concat_axis=1, tiled=True)
    return mixed[None]


def solution(mesh):
    placed = (P("dp", "sp", None), P("dp", None), P("dp", None), P("dp", None), P(), P())
    return jax.shard_map(
        on_device, mesh=mesh, in_specs=placed, out_specs=P("dp", "sp", None), check_vma=False
    )
```

profile of v0, /device:TPU:1, one launch (start us, length us, event | category | flops | bytes accessed | tf_op | source)
XLA Modules:
  0.0 497.8 jit_solution(16956507207501751154)
XLA Ops:
  10.2 15.7 %all-to-all-start.1 = ((bf16[192,16,1]{0,2,1:T(2,128)(2,1)}), bf16[192,16,1]{0,2,1:T(2,128)(2,1)S(1)}, u32[]{:S(2)}, u32[]{:S(2)}) async-start(bf16[192,16,1]{0,2,1:T(2,128)(2,1)} %copy.24), calls=%async_computation.1 | async-start | bytes 32768 | tf_op jit(solution)/shard_map/all_to_all | solution.py:55
  26.0 68.4 %all-gather.2.cloned.1.call-done = bf16[2048,3072]{1,0:T(8,128)(2,1)} async-done(((bf16[64,3072]{1,0:T(8,128)(2,1)}), bf16[2048,3072]{1,0:T(8,128)(2,1)}) %all-gather.2.cloned.1.call-update) | async-done | bytes 12582928 | tf_op jit(solution)/shard_map/all_gather | solution.py:13
  94.3 5.2 %fusion.31 = bf16[24,16,8,128]{3,2,1,0:T(8,128)(2,1)S(1)} fusion(bf16[2048,3072]{1,0:T(8,128)(2,1)} %all-gather.2.cloned.1.call-done, bf16[1,192,2048]{2,1,0:T(8,128)(2,1)S(1)} %copy-done), kind=kOutput, calls=%fused_computation.39 | convolution fusion | flops 1611005952 | bytes 9961472 | tf_op jit(solution)/shard_map/dot_general | solution.py:34
  100.7 12.1 %all-to-all-start = ((bf16[192,16,128]{2,0,1:T(8,128)(2,1)}), bf16[192,16,128]{2,0,1:T(8,128)(2,1)}, u32[]{:S(2)}, u32[]{:S(2)}) async-start(bf16[192,16,128]{2,0,1:T(8,128)(2,1)} %bitcast.116), calls=%async_computation | async-start | bytes 1572864 | tf_op jit(solution)/shard_map/all_to_all | solution.py:52
  115.0 32.2 %all-to-all-done = bf16[192,16,128]{2,0,1:T(8,128)(2,1)} async-done(((bf16[192,16,128]{2,0,1:T(8,128)(2,1)}), bf16[192,16,128]{2,0,1:T(8,128)(2,1)}, u32[]{:S(2)}, u32[]{:S(2)}) %all-to-all-start) | async-done | bytes 786464 | tf_op jit(solution)/shard_map/all_to_all | solution.py:52
  148.2 12.5 %all-to-all-start.2 = ((bf16[192,16,128]{2,0,1:T(8,128)(2,1)}), bf16[192,16,128]{2,0,1:T(8,128)(2,1)}, u32[]{:S(2)}, u32[]{:S(2)}) async-start(bf16[192,16,128]{2,0,1:T(8,128)(2,1)} %bitcast.17), calls=%async_computation.2 | async-start | bytes 1572864 | tf_op jit(solution)/shard_map/all_to_all | solution.py:53
  162.9 32.4 %all-to-all-done.2 = bf16[192,16,128]{2,0,1:T(8,128)(2,1)} async-done(((bf16[192,16,128]{2,0,1:T(8,128)(2,1)}), bf16[192,16,128]{2,0,1:T(8,128)(2,1)}, u32[]{:S(2)}, u32[]{:S(2)}) %all-to-all-start.2) | async-done | bytes 786464 | tf_op jit(solution)/shard_map/all_to_all | solution.py:53
  196.3 12.3 %all-to-all-start.3 = ((bf16[192,16,128]{2,0,1:T(8,128)(2,1)}), bf16[192,16,128]{2,0,1:T(8,128)(2,1)}, u32[]{:S(2)}, u32[]{:S(2)}) async-start(bf16[192,16,128]{2,0,1:T(8,128)(2,1)} %bitcast.21), calls=%async_computation.3 | async-start | bytes 1572864 | tf_op jit(solution)/shard_map/all_to_all | solution.py:54
  209.5 33.7 %all-to-all-done.3 = bf16[192,16,128]{2,0,1:T(8,128)(2,1)} async-done(((bf16[192,16,128]{2,0,1:T(8,128)(2,1)}), bf16[192,16,128]{2,0,1:T(8,128)(2,1)}, u32[]{:S(2)}, u32[]{:S(2)}) %all-to-all-start.3) | async-done | bytes 786464 | tf_op jit(solution)/shard_map/all_to_all | solution.py:54
  243.3 198.2 %while.39 = (s32[]{:T(128)}, bf16[6,512,128]{2,1,0:T(8,128)(2,1)}, s32[6]{0:T(128)S(1)}, bf16[3072,1,1,128]{3,0,2,1:T(8,128)(2,1)}, f32[1,1,3072]{2,1,0:T(1,128)...) while((s32[]{:T(128)}, bf16[6,512,128]{2,1,0:T(8,128)(2,1)}, ...), condition=%wide.region_9.10_spmd.clone.clone, body=%wide.region_2.0_spmd.clone.clone.sunk | while | flops 141164576 | bytes 27561412 | solution.py:121
  246.3 3.5 broadcast.130
  249.7 2.2 while.40
  249.7 2.2 fusion.67
  252.0 3.2 reduce_max.20
  255.2 3.7 exponential_reduce_fusion.2
  258.9 3.1 while.41
  265.9 3.5 broadcast.130
  269.4 4.5 while.40
  271.6 2.3 fusion.67
  273.9 3.2 reduce_max.20
  277.1 3.7 exponential_reduce_fusion.2
  280.9 6.2 %while.41 = (s32[]{:T(128)}, f32[512,1,1,128]{0,3,2,1:T(8,128)S(1)}, s32[]{:T(128)}, bf16[3072,1,128]{2,0,1:T(8,128)(2,1)}, f32[6,1,1,512,512]{3,4,2,1,0:T(8,128...) while((s32[]{:T(128)}, ...), condition=%wide.region_8.8_spmd, body=%wide.region_7.7_spmd.sunk | while | flops 67960840 | bytes 5902541 | solution.py:113
  290.9 3.5 broadcast.130
  294.4 6.8 %while.40 = (s32[]{:T(128)}, f32[6,1,1,512,512]{3,4,2,1,0:T(8,128)}, s32[]{:T(128)}, s32[512]{0:T(512)S(1)}, s32[]{:T(128)}, /*index=5*/bf16[3072,1,128]{2,0,1:T...) while((s32[]{:T(128)}, ...), condition=%wide.region_4.4_spmd.clone, body=%wide.region_3.3_spmd.clone.sunk | while | flops 68420616 | bytes 1329385 | solution.py:88
  296.6 2.3 fusion.67
  301.1 3.2 reduce_max.20
  304.4 3.7 exponential_reduce_fusion.2
  308.1 9.3 %while.41 = (s32[]{:T(128)}, f32[512,1,1,128]{0,3,2,1:T(8,128)S(1)}, s32[]{:T(128)}, bf16[3072,1,128]{2,0,1:T(8,128)(2,1)}, f32[6,1,1,512,512]{3,4,2,1,0:T(8,128...) while((s32[]{:T(128)}, ...), condition=%wide.region_8.8_spmd, body=%wide.region_7.7_spmd.sunk | while | flops 67960840 | bytes 5902541 | solution.py:113
  321.3 3.5 broadcast.130
  324.7 9.0 %while.40 = (s32[]{:T(128)}, f32[6,1,1,512,512]{3,4,2,1,0:T(8,128)}, s32[]{:T(128)}, s32[512]{0:T(512)S(1)}, s32[]{:T(128)}, /*index=5*/bf16[3072,1,128]{2,0,1:T...) while((s32[]{:T(128)}, ...), condition=%wide.region_4.4_spmd.clone, body=%wide.region_3.3_spmd.clone.sunk | while | flops 68420616 | bytes 1329385 | solution.py:88
  327.0 2.3 fusion.67
  333.7 3.2 reduce_max.20
  337.0 3.7 exponential_reduce_fusion.2
  340.7 12.4 %while.41 = (s32[]{:T(128)}, f32[512,1,1,128]{0,3,2,1:T(8,128)S(1)}, s32[]{:T(128)}, bf16[3072,1,128]{2,0,1:T(8,128)(2,1)}, f32[6,1,1,512,512]{3,4,2,1,0:T(8,128...) while((s32[]{:T(128)}, ...), condition=%wide.region_8.8_spmd, body=%wide.region_7.7_spmd.sunk | while | flops 67960840 | bytes 5902541 | solution.py:113
  357.0 3.5 broadcast.130
  360.5 11.2 %while.40 = (s32[]{:T(128)}, f32[6,1,1,512,512]{3,4,2,1,0:T(8,128)}, s32[]{:T(128)}, s32[512]{0:T(512)S(1)}, s32[]{:T(128)}, /*index=5*/bf16[3072,1,128]{2,0,1:T...) while((s32[]{:T(128)}, ...), condition=%wide.region_4.4_spmd.clone, body=%wide.region_3.3_spmd.clone.sunk | while | flops 68420616 | bytes 1329385 | solution.py:88
  362.7 2.3 fusion.67
  371.7 3.2 reduce_max.20
  374.9 3.7 exponential_reduce_fusion.2
  378.6 15.6 %while.41 = (s32[]{:T(128)}, f32[512,1,1,128]{0,3,2,1:T(8,128)S(1)}, s32[]{:T(128)}, bf16[3072,1,128]{2,0,1:T(8,128)(2,1)}, f32[6,1,1,512,512]{3,4,2,1,0:T(8,128...) while((s32[]{:T(128)}, ...), condition=%wide.region_8.8_spmd, body=%wide.region_7.7_spmd.sunk | while | flops 67960840 | bytes 5902541 | solution.py:113
  398.0 3.5 broadcast.130
  401.5 13.5 %while.40 = (s32[]{:T(128)}, f32[6,1,1,512,512]{3,4,2,1,0:T(8,128)}, s32[]{:T(128)}, s32[512]{0:T(512)S(1)}, s32[]{:T(128)}, /*index=5*/bf16[3072,1,128]{2,0,1:T...) while((s32[]{:T(128)}, ...), condition=%wide.region_4.4_spmd.clone, body=%wide.region_3.3_spmd.clone.sunk | while | flops 68420616 | bytes 1329385 | solution.py:88
  403.7 2.3 fusion.67
  412.7 2.3 fusion.67
  415.0 3.2 reduce_max.20
  418.3 3.7 exponential_reduce_fusion.2
  422.0 18.7 %while.41 = (s32[]{:T(128)}, f32[512,1,1,128]{0,3,2,1:T(8,128)S(1)}, s32[]{:T(128)}, bf16[3072,1,128]{2,0,1:T(8,128)(2,1)}, f32[6,1,1,512,512]{3,4,2,1,0:T(8,128...) while((s32[]{:T(128)}, ...), condition=%wide.region_8.8_spmd, body=%wide.region_7.7_spmd.sunk | while | flops 67960840 | bytes 5902541 | solution.py:113
  441.5 47.8 %all_to_all.77 = bf16[16,192,128]{2,1,0:T(8,128)(2,1)S(1)} all-to-all(bf16[16,192,128]{2,1,0:T(8,128)(2,1)} %bitcast.157), channel_id=1, replica_groups=mesh['sp'=16,'dp'=32] {'sp'}, dimensions={0} | all-to-all | bytes 1572864 | tf_op jit(solution)/shard_map/all_to_all | solution.py:123
  (194 shorter events, 124.0 us)
Async XLA Ops:
  6.5 1.9 copy-start
  6.5 87.8 %all-gather.2.cloned.1.call-start = ((), (), s32[]{:S(2)}) async-start(), calls=%async_computation.5 | async-start | bytes 12976128 | tf_op jit(solution)/shard_map/all_gather | solution.py:13
  10.2 90.4 %all-to-all-start.1 = ((bf16[192,16,1]{0,2,1:T(2,128)(2,1)}), bf16[192,16,1]{0,2,1:T(2,128)(2,1)S(1)}, u32[]{:S(2)}, u32[]{:S(2)}) async-start(bf16[192,16,1]{0,2,1:T(2,128)(2,1)} %copy.24), calls=%async_computation.1 | async-start | bytes 32768 | tf_op jit(solution)/shard_map/all_to_all | solution.py:55
  100.7 46.4 %all-to-all-start = ((bf16[192,16,128]{2,0,1:T(8,128)(2,1)}), bf16[192,16,128]{2,0,1:T(8,128)(2,1)}, u32[]{:S(2)}, u32[]{:S(2)}) async-start(bf16[192,16,128]{2,0,1:T(8,128)(2,1)} %bitcast.116), calls=%async_computation | async-start | bytes 1572864 | tf_op jit(solution)/shard_map/all_to_all | solution.py:52
  148.2 47.2 %all-to-all-start.2 = ((bf16[192,16,128]{2,0,1:T(8,128)(2,1)}), bf16[192,16,128]{2,0,1:T(8,128)(2,1)}, u32[]{:S(2)}, u32[]{:S(2)}) async-start(bf16[192,16,128]{2,0,1:T(8,128)(2,1)} %bitcast.17), calls=%async_computation.2 | async-start | bytes 1572864 | tf_op jit(solution)/shard_map/all_to_all | solution.py:53
  196.3 46.9 %all-to-all-start.3 = ((bf16[192,16,128]{2,0,1:T(8,128)(2,1)}), bf16[192,16,128]{2,0,1:T(8,128)(2,1)}, u32[]{:S(2)}, u32[]{:S(2)}) async-start(bf16[192,16,128]{2,0,1:T(8,128)(2,1)} %bitcast.21), calls=%async_computation.3 | async-start | bytes 1572864 | tf_op jit(solution)/shard_map/all_to_all | solution.py:54
Sparse Core Ops, SparseCore 0:
  10.5 83.8 all-gather.1
where the time goes:
time: 506 us; the launch traced here: 498 us
  waiting for transfers between devices  167 us (33%)
  matrix products  88 us (17%)
  local copies, waits for them, and re-layouts  75.3 us (15%)
  starting transfers between devices  52.6 us (10%)
  blocking collectives  47.8 us (9%)
  other arithmetic  44.2 us (9%)
  between operations  13.5 us (3%)
  loops' own time  9.76 us (2%)
    all_gather x1, waiting for transfers between devices, in_one_piece(): lax.all_gather(both, axis, axis=dim, tiled=True)  68.4 us
    all_to_all x1, blocking collectives, on_device(): lax.all_to_all(head_mixed, 'sp', split_axis=0, concat_axis=1, tiled=True)  47.8 us
    dot_general x21, matrix products, fill_scores(): jnp.einsum('qkgd,skd->kgqs', query_part, key_part, preferred_element_type...  47.1 us
    dynamic_slice x42, local copies, waits for them, and re-layouts, weighted(): lax.dynamic_index_in_dim(score_buffer, key_block, 0, keepdims=False)  34.2 us
    all_to_all x1, waiting for transfers between devices, on_device(): lax.all_to_all(value_rows, 'sp', split_axis=1, concat_axis=0, tiled=True)  33.7 us
    all_to_all x1, waiting for transfers between devices, on_device(): lax.all_to_all(key_rows, 'sp', split_axis=1, concat_axis=0, tiled=True)  32.4 us
    all_to_all x1, waiting for transfers between devices, on_device(): lax.all_to_all(query_rows, 'sp', split_axis=1, concat_axis=0, tiled=True)  32.2 us
    dot_general x21, matrix products, weighted(): jnp.einsum('kgqs,skd->qkgd', weights, value_part, preferred_element_type=...  30.1 us
  transfers between devices with their start and end apart: 5, of which 4 were waited for; matrix products, arithmetic and copies ran while one was open for 3% of the time, Pallas kernels for 0%

commit v1 on v0

v1 whole, which is shorter than its diff:
```python
import functools
import math

import jax
import jax.numpy as jnp
from jax import lax
from jax.experimental import pallas as pl
from jax.experimental.pallas import tpu as pltpu
from jax.sharding import PartitionSpec as P

BF16 = jnp.bfloat16
F32 = jnp.float32
MESH = pl.DeviceIdType.MESH
SIDE = 4
KEYS, VALUES, GATES = 0, 1, 2
UP, DOWN = 0, 1
NT = (((1,), (1,)), ((), ()))
TN = (((0,), (0,)), ((), ()))

WHOLE = [("W", 1, 0), ("W", 3, 0), ("W", 0, 1), ("W", 0, 3), ("W", 2, 0), ("W", 0, 2)]
HALVES = [(part, a, b) for part in "AB" for a in (1, 2, 3) for b in (1, 2, 3)]
ITEM = {key: n for n, key in enumerate(WHOLE + HALVES)}


class Gather:
    def __init__(self, number, shard, full, local_sem, sends, receives, pair_sends, pair_receives, place):
        self.number, self.shard, self.full, self.local_sem = number, shard, full, local_sem
        self.sems = (sends, receives, pair_sends, pair_receives)
        self.place = place
        self.depth = shard.shape[0]
        self.started = []

    def slot(self, a, b, other=False):
        x, y, core, turn = self.place
        if other:
            core, turn = 1 - core, -turn
        across = lax.rem(x + turn * a + 2 * SIDE, SIDE)
        along = lax.rem(y + turn * b + 2 * SIDE, SIDE)
        return (along * SIDE + across) * 2 + core

    def rows(self, key, other=False):
        part, a, b = key
        first = self.slot(a, b, other) * self.depth
        count = self.depth if part == "W" else self.depth // 2
        if part == "B":
            first = first + count
        return self.full.at[pl.ds(pl.multiple_of(first, count), count)]

    def copy(self, key, received, target):
        sends, receives = self.sems[:2]
        n = ITEM[received]
        view = self.rows(key)
        return pltpu.make_async_remote_copy(
            src_ref=view,
            dst_ref=view,
            send_sem=sends.at[self.number, n],
            recv_sem=receives.at[self.number, n],
            device_id={"dp": target},
            device_id_type=MESH,
        )

    def send(self, key, dx, dy):
        part, a, b = key
        received = (part, (a - dx) % SIDE, (b - dy) % SIDE)
        copy = self.copy(key, received, self.slot(dx, dy))
        copy.start()
        self.started.append(copy)

    def wait(self, key):
        self.copy(key, key, self.slot(1, 0)).wait_recv()

    def pair_copy(self, a, b, other=False):
        x, y, core, turn = self.place
        view = self.rows(("W", a, b), other)
        return pltpu.make_async_remote_copy(
            src_ref=view,
            dst_ref=view,
            send_sem=self.sems[2].at[self.number, a * SIDE + b],
            recv_sem=self.sems[3].at[self.number, a * SIDE + b],
            device_id={"dp": (y * SIDE + x) * 2 + 1 - core},
            device_id_type=MESH,
        )

    def share(self, a, b):
        copy = self.pair_copy(a, b)
        copy.start()
        self.started.append(copy)

    def fetch(self):
        self.fetched = pltpu.make_async_copy(self.shard, self.rows(("W", 0, 0)), self.local_sem.at[self.number])
        self.fetched.start()

    def begin(self):
        self.fetched.wait()
        for dx, dy in ((1, 0), (0, 1), (-1, 0), (0, -1)):
            self.send(("W", 0, 0), dx, dy)
        self.share(0, 0)

    def first(self):
        for a in (3, 1):
            self.wait(("W", a, 0))
            if a == 3:
                self.send(("W", 3, 0), 1, 0)
            for dy in (1, -1):
                self.send(("A", a, 0), 0, dy)
            self.wait(("W", 0, a))
            if a == 3:
                self.send(("W", 0, 3), 0, 1)
            for dx in (1, -1):
                self.send(("B", 0, a), dx, 0)
            self.share(a, 0)
            self.share(0, a)

    def second(self):
        for a in (3, 1):
            self.wait(("A", a, 3))
            self.send(("A", a, 3), 0, 1)
            self.wait(("B", 3, a))
            self.send(("B", 3, a), 1, 0)
        self.wait(("W", 2, 0))
        for dy in (1, -1):
            self.send(("A", 2, 0), 0, dy)
        self.wait(("W", 0, 2))
        for dx in (1, -1):
            self.send(("B", 0, 2), dx, 0)
        self.share(2, 0)
        self.share(0, 2)
        for a in (3, 1):
            self.wait(("A", a, 1))
            self.wait(("B", 1, a))
        for a in (3, 1):
            for b in (3, 1):
                self.share(a, b)

    def third(self):
        self.wait(("A", 2, 3))
        self.send(("A", 2, 3), 0, 1)
        self.wait(("B", 3, 2))
        self.send(("B", 3, 2), 1, 0)
        for a in (3, 1):
            self.wait(("A", a, 2))
            self.wait(("B", 2, a))
        self.wait(("A", 2, 1))
        self.wait(("B", 1, 2))
        for a in (3, 1):
            self.share(2, a)
            self.share(a, 2)

    def fourth(self):
        self.wait(("A", 2, 2))
        self.wait(("B", 2, 2))
        self.share(2, 2)

    def complete(self):
        for a in range(SIDE):
            for b in range(SIDE):
                self.pair_copy(a, b, other=True).wait_recv()

    def drain(self):
        for copy in self.started:
            copy.wait_send()


def kernel(
    tokens, query_shard, key_shard, value_shard, forget_weight, forget_bias, out,
    query_all, key_all, value_all, keys, values, gates, key_extra, queries, totals, peaks, sums,
    local_sem, sends, receives, pair_sends, pair_receives, ring_sends, ring_receives,
):
    ring = lax.axis_size("sp")
    half = ring // 2
    me = lax.axis_index("sp")
    mine = lax.axis_index("dp")
    core = lax.rem(mine, 2)
    x = lax.rem(lax.div(mine, 2), SIDE)
    y = lax.div(mine, 2 * SIDE)
    place = (x, y, core, 1 - 2 * core)
    rows = tokens.shape[0]
    heads = forget_weight.shape[1]
    groups, dim = keys.shape[1], keys.shape[3]
    share = heads // groups
    root = math.sqrt(dim)

    gather_keys, gather_values, gather_queries = (
        Gather(n, shard, full, local_sem, sends, receives, pair_sends, pair_receives, place)
        for n, (shard, full) in enumerate(
            ((key_shard, key_all), (value_shard, value_all), (query_shard, query_all))
        )
    )
    for g in (gather_keys, gather_values, gather_queries):
        g.fetch()

    above, below = lax.rem(me + 1, ring), lax.rem(me + ring - 1, ring)
    barrier = pltpu.get_barrier_semaphore()
    for dx, dy in ((1, 0), (0, 1), (-1, 0), (0, -1)):
        pl.semaphore_signal(
            barrier, inc=1, device_id={"dp": gather_keys.slot(dx, dy)}, device_id_type=MESH
        )
    pl.semaphore_signal(barrier, inc=1, device_id={"dp": mine + 1 - 2 * core}, device_id_type=MESH)
    for neighbour in (above, below):
        pl.semaphore_signal(barrier, inc=1, device_id={"sp": neighbour}, device_id_type=MESH)
    pl.semaphore_wait(barrier, 7)

    buffers = {KEYS: keys, VALUES: values, GATES: gates}
    last = {
        (KEYS, UP): half, (KEYS, DOWN): half - 1,
        (VALUES, UP): half - 1, (VALUES, DOWN): half,
        (GATES, UP): half, (GATES, DOWN): half - 1,
    }

    def hop(kind, way, step, slot):
        view = buffers[kind].at[slot]
        return pltpu.make_async_remote_copy(
            src_ref=view,
            dst_ref=view,
            send_sem=ring_sends.at[kind, way, step - 1],
            recv_sem=ring_receives.at[kind, way, step - 1],
            device_id={"sp": above if way == UP else below},
            device_id_type=MESH,
        )

    def origin(way, step):
        return lax.rem(me - step + ring, ring) if way == UP else lax.rem(me + step, ring)

    def launch(kind):
        for way in (UP, DOWN):
            hop(kind, way, 1, me).start()

    def relay(kind, step):
        for way in (UP, DOWN):
            final = last[kind, way]
            slot = origin(way, step)
            if isinstance(step, int):
                if step <= final:
                    hop(kind, way, step, slot).wait_recv()
                if step < final:
                    hop(kind, way, step + 1, slot).start()
            else:
                hop(kind, way, step, slot).wait_recv()

                @pl.when(step < final)
                def _():
                    hop(kind, way, step + 1, slot).start()

    gather_keys.begin()
    gather_values.begin()

    wide = gates.shape[2]
    gate_input = jnp.dot(tokens[...], forget_weight[...], preferred_element_type=F32) + forget_bias[...]
    log_gate = (jnp.minimum(gate_input, 0.0) - jnp.log1p(jnp.exp(-jnp.abs(gate_input)))).astype(BF16)
    eye = (
        lax.broadcasted_iota(jnp.int32, (rows, wide), 0) == lax.broadcasted_iota(jnp.int32, (rows, wide), 1)
    ).astype(F32).astype(BF16)
    gates[me] = lax.dot_general(log_gate, eye, TN, preferred_element_type=F32).astype(BF16)

    gather_keys.first()
    launch(GATES)
    gather_values.first()
    relay(GATES, 1)
    gather_keys.second()
    relay(GATES, 2)
    gather_values.second()
    gather_keys.third()
    relay(GATES, 3)
    gather_queries.begin()
    gather_keys.fourth()
    relay(GATES, 4)
    gather_keys.complete()

    def project(weight, block):
        def one(g, carry):
            columns = pl.ds(pl.multiple_of(g * dim * 2, dim * 2), dim * 2)
            part = jnp.dot(tokens[...], weight[:, columns], preferred_element_type=F32).astype(BF16)
            block[me, 2 * g] = part[:, :dim]
            block[me, 2 * g + 1] = part[:, dim:]
            return carry

        lax.fori_loop(0, groups // 2, one, 0)

    project(key_all, keys)
    gather_values.third()
    launch(KEYS)
    relay(GATES, 5)
    gather_values.fourth()
    gather_values.complete()
    project(value_all, values)
    relay(GATES, 6)
    launch(VALUES)
    gather_queries.first()
    relay(GATES, 7)
    relay(GATES, 8)

    lane = lax.broadcasted_iota(jnp.int32, (rows, dim), 1)
    tall = rows + 8
    down = lax.broadcasted_iota(jnp.int32, (tall, wide), 0)
    right = lax.broadcasted_iota(jnp.int32, (tall, wide), 1)
    later = ((right > down) | (down >= rows)).astype(F32).astype(BF16)
    sofar = ((right <= down) & (down < rows)).astype(F32).astype(BF16)

    def thrice(block):
        g = gates[block]
        return jnp.concatenate([g, g, g, jnp.zeros((dim - 3 * heads, wide), BF16)], axis=0)

    def parts(exact):
        hi = exact.astype(BF16).astype(F32)
        rest = exact - hi
        mid = rest.astype(BF16).astype(F32)
        low = rest - mid
        return jnp.where(
            lane < heads, hi, jnp.where(lane < 2 * heads, mid, jnp.where(lane < 3 * heads, low, 0.0))
        )

    ones = ((lane >= 3 * heads) & (lane < 3 * heads + 3)).astype(F32)

    def decay_of(step, after):
        block = lax.rem(me - step + ring, ring)
        summed = lax.dot_general(later, thrice(block), NT, preferred_element_type=F32)
        key_extra[block] = (parts((summed[:rows] + after) * root) + ones).astype(BF16)
        return after + summed[rows : rows + 1]

    own = lax.dot_general(later, thrice(me), NT, preferred_element_type=F32)[rows : rows + 1]
    lax.fori_loop(0, ring, decay_of, -own)

    own_sum = lax.dot_general(sofar, thrice(me), NT, preferred_element_type=F32)[:rows]
    own_parts = parts(own_sum * root).astype(BF16)
    pick_row = lax.broadcasted_iota(jnp.int32, (dim, dim), 0)
    pick_lane = lax.broadcasted_iota(jnp.int32, (dim, dim), 1)

    def query_extra(h, carry):
        pick = ((pick_row == h + heads * (pick_lane - 3 * heads)) & (pick_lane >= 3 * heads)
                & (pick_lane < 3 * heads + 3)).astype(F32).astype(BF16)
        moved = jnp.dot(own_parts, pick, preferred_element_type=F32)
        hot = ((lane == h) | (lane == h + heads) | (lane == h + 2 * heads)).astype(F32)
        place_rows = pl.ds(pl.multiple_of(lax.rem(h, share) * rows, rows), rows)
        queries[lax.div(h, share), place_rows, dim:] = (moved + hot).astype(BF16)
        return carry

    lax.fori_loop(0, heads, query_extra, 0)

    relay(KEYS, 1)
    relay(VALUES, 1)
    gather_queries.second()
    relay(KEYS, 2)
    relay(VALUES, 2)
    gather_queries.third()
    relay(KEYS, 3)
    gather_queries.fourth()
    relay(VALUES, 3)
    gather_queries.complete()

    def query_group(g, carry):
        columns = pl.ds(pl.multiple_of(g * dim * share, dim * share), dim * share)
        part = jnp.dot(tokens[...], query_all[:, columns], preferred_element_type=F32).astype(BF16)
        for h in range(share):
            queries[g, h * rows : (h + 1) * rows, :dim] = part[:, h * dim : (h + 1) * dim]
        return carry

    lax.fori_loop(0, groups, query_group, 0)

    scale = 1.0 / root
    breadth = share * rows

    def attend(block, diagonal=False):
        def one(g, carry):
            key_part = jnp.concatenate([keys[block, g], key_extra[block]], axis=1)
            score = lax.dot_general(key_part, queries[g], NT, preferred_element_type=F32) * scale
            if diagonal:
                key_at = lax.broadcasted_iota(jnp.int32, (rows, breadth), 0)
                query_at = lax.broadcasted_iota(jnp.int32, (rows, breadth), 1)
                for h in range(share - 1, 0, -1):
                    query_at = jnp.where(query_at >= h * rows, query_at - h * rows, query_at)
                score = jnp.where(key_at <= query_at, score, -jnp.inf)
                peak = jnp.max(score, axis=0, keepdims=True)
            else:
                old = peaks[g]
                peak = jnp.maximum(old, jnp.max(score, axis=0, keepdims=True))
            weight = jnp.exp(score - peak)
            total = jnp.sum(weight, axis=0, keepdims=True)
            mixed = lax.dot_general(values[block, g], weight.astype(BF16), TN, preferred_element_type=F32)
            peaks[g] = peak
            if diagonal:
                sums[g] = total
                totals[g] = mixed
            else:
                fade = jnp.exp(old - peak)
                sums[g] = sums[g] * fade + total
                totals[g] = totals[g] * fade + mixed
            return carry

        lax.fori_loop(0, groups, one, 0)

    def unit(u):
        step = lax.div(u, 2) + 1
        upward = lax.rem(u, 2) == 0
        block = jnp.where(upward, me - step, me + step - ring)

        @pl.when(block >= 0)
        def _():
            attend(block)

    attend(me, diagonal=True)

    def steady(step, carry):
        relay(KEYS, step)
        unit(3 * (step - 4))
        unit(3 * (step - 4) + 1)
        relay(VALUES, step)
        unit(3 * (step - 4) + 2)
        return carry

    lax.fori_loop(4, half, steady, 0)
    relay(KEYS, half)
    for u in range(3 * (half - 4), 2 * (half - 1)):
        unit(u)
    relay(VALUES, half)

    @pl.when(me >= half)
    def _():
        attend(me - half)

    for g in range(groups):
        mixed = (totals[g] / sums[g]).T
        for h in range(share):
            at = (g * share + h) * dim
            out[:, at : at + dim] = mixed[h * rows : (h + 1) * rows].astype(BF16)

    for g in (gather_keys, gather_values, gather_queries):
        g.drain()
    for kind in (KEYS, VALUES, GATES):
        for way in (UP, DOWN):
            def sent(n, carry, kind=kind, way=way):
                hop(kind, way, n + 1, me).wait_send()
                return carry

            lax.fori_loop(0, last[kind, way], sent, 0)


def on_device(tokens, query_weight, key_weight, value_weight, forget_weight, forget_bias):
    token_rows = tokens[0]
    rows, width = token_rows.shape
    ring = lax.axis_size("sp")
    heads = forget_weight.shape[1]
    dim = query_weight.shape[1] // heads
    groups = key_weight.shape[1] // dim
    share = heads // groups
    wide = -(-rows // 128) * 128
    vmem = pl.BlockSpec(memory_space=pltpu.VMEM)
    anywhere = pl.BlockSpec(memory_space=pl.ANY)
    mixed = pl.pallas_call(
        kernel,
        out_shape=jax.ShapeDtypeStruct((rows, heads * dim), BF16),
        in_specs=[vmem, anywhere, anywhere, anywhere, vmem, vmem],
        out_specs=vmem,
        scratch_shapes=[
            pltpu.VMEM((width, heads * dim), BF16),
            pltpu.VMEM((width, groups * dim), BF16),
            pltpu.VMEM((width, groups * dim), BF16),
            pltpu.VMEM((ring, groups, rows, dim), BF16),
            pltpu.VMEM((ring, groups, rows, dim), BF16),
            pltpu.VMEM((ring, heads, wide), BF16),
            pltpu.VMEM((ring, rows, dim), BF16),
            pltpu.VMEM((groups, share * rows, 2 * dim), BF16),
            pltpu.VMEM((groups, dim, share * rows), F32),
            pltpu.VMEM((groups, 1, share * rows), F32),
            pltpu.VMEM((groups, 1, share * rows), F32),
            pltpu.SemaphoreType.DMA((3,)),
            pltpu.SemaphoreType.DMA((3, len(ITEM))),
            pltpu.SemaphoreType.DMA((3, len(ITEM))),
            pltpu.SemaphoreType.DMA((3, SIDE * SIDE)),
            pltpu.SemaphoreType.DMA((3, SIDE * SIDE)),
            pltpu.SemaphoreType.DMA((3, 2, ring // 2)),
            pltpu.SemaphoreType.DMA((3, 2, ring // 2)),
        ],
        compiler_params=pltpu.CompilerParams(
            collective_id=0, has_side_effects=True, vmem_limit_bytes=60 * 2**20
        ),
    )(token_rows, query_weight, key_weight, value_weight, forget_weight, forget_bias[None, :])
    return mixed[None]


def solution(mesh):
    placed = (P("dp", "sp", None), P("dp", None), P("dp", None), P("dp", None), P(), P())
    return jax.shard_map(
        on_device, mesh=mesh, in_specs=placed, out_specs=P("dp", "sp", None), check_vma=False
    )
```

time: 506 us -> 117 us (0.23); the launches traced: 498 us -> 116 us
  waiting for transfers between devices: 167 us -> 0 us
  Pallas kernels: 0 us -> 112 us
  matrix products: 88 us -> 0 us
  local copies, waits for them, and re-layouts: 75.3 us -> 3.93 us
  starting transfers between devices: 52.6 us -> 0 us
  blocking collectives: 47.8 us -> 0 us
  other arithmetic: 44.2 us -> 0 us
  between operations: 13.5 us -> 0.01 us
  loops' own time: 9.76 us -> 0 us
    pallas_call x0 -> x1, Pallas kernels: none -> 112 us  [on_device(): pl.pallas_call(kernel, out_shape=jax.ShapeDtypeStruct((rows, heads * dim)...]
    all_to_all x4 -> x0, waiting for transfers between devices: 98.3 us -> none  [the longest x1 33.7 us: on_device(): lax.all_to_all(value_rows, 'sp', split_axis=1, concat_axis=0, tiled=True)]
    dot_general x46 -> x0, matrix products: 88 us -> none  [the longest x21 47.1 us: fill_scores(): jnp.einsum('qkgd,skd->kgqs', query_part, key_part, preferred_element_type...]
    all_gather x1 -> x0, waiting for transfers between devices: 68.4 us -> none  [in_one_piece(): lax.all_gather(both, axis, axis=dim, tiled=True)]
    all_to_all x4 -> x0, starting transfers between devices: 52.6 us -> none  [the longest x1 15.7 us: on_device(): lax.all_to_all(log_gate, 'sp', split_axis=1, concat_axis=0, tiled=True)]
    all_to_all x1 -> x0, blocking collectives: 47.8 us -> none  [on_device(): lax.all_to_all(head_mixed, 'sp', split_axis=0, concat_axis=1, tiled=True)]
    dynamic_slice x81 -> x0, local copies, waits for them, and re-layouts: 43.8 us -> none  [the longest x42 34.2 us: weighted(): lax.dynamic_index_in_dim(score_buffer, key_block, 0, keepdims=False)]
    reduce_sum x6 -> x0, other arithmetic: 22.1 us -> none  [query_block(): jnp.sum(jnp.sum(jnp.exp(score_buffer - row_max[None, ..., None]), axis=-1...]
  transfers between devices with their start and end apart: 5 -> 0, of which waited for: 4 -> 0; matrix products, arithmetic and copies ran while one was open for 3% -> 0% of each run, Pallas kernels for 0% -> 0%
where the time goes in v1:
time: 117 us; the launch traced here: 116 us
  Pallas kernels  112 us (96%)
  local copies, waits for them, and re-layouts  3.93 us (3%)
    pallas_call x1, Pallas kernels, on_device(): pl.pallas_call(kernel, out_shape=jax.ShapeDtypeStruct((rows, heads * dim)...  112 us
    unnamed x2, local copies, waits for them, and re-layouts  3.93 us

profile of v1, /device:TPU:1, one launch (start us, length us, event | category | flops | bytes accessed | tf_op | source)
XLA Modules:
  0.0 116.0 jit_solution(2996545438724987541)
XLA Ops:
  0.0 1.8 %copy.7.forget_weight = bf16[2048,16]{1,0:T(8,128)(2,1)} copy(bf16[2048,16]{0,1:T(8,128)(2,1)} %param.10) | data formatting | bytes 131072 | tf_op args[4]
  1.8 112.0 %shard_map.64 = bf16[192,2048]{1,0:T(8,128)(2,1)} custom-call(bf16[192,2048]{1,0:T(8,128)(2,1)} %bitcast.4, bf16[64,2048]{1,0:T(8,128)(2,1)} %query_shard.1, bf16[64,512]{1,0:T(8,128)(2,1)} %key_shard.1, bf16[64,512]{1,0:T(8,128)(2,1)} %value_shard.1, bf16[2048,16]{1,0:T(8,128)(2,1)} %copy.7.forget_weight, f32[1,16]{1,0:T(1,128)} %bitcast.5), custom_call_target="tpu_custom_call" | custom-call | tf_op jit(solution)/shard_map/pallas_call | solution.py:448
  113.9 2.1 %copy.9 = bf16[1,192,2048]{2,1,0:T(8,128)(2,1)} copy(bf16[1,192,2048]{2,1,0:T(8,128)(2,1)} %bitcast.3) | data formatting | bytes 1572864

commit v2 on v1

v2 whole, which is shorter than its diff:
```python
import functools
import math

import jax
import jax.numpy as jnp
from jax import lax
from jax.experimental import pallas as pl
from jax.experimental.pallas import tpu as pltpu
from jax.sharding import PartitionSpec as P

BF16 = jnp.bfloat16
F32 = jnp.float32
MESH = pl.DeviceIdType.MESH
SIDE = 4
KEYS, VALUES, GATES = 0, 1, 2
UP, DOWN = 0, 1
NT = (((1,), (1,)), ((), ()))
TN = (((0,), (0,)), ((), ()))

WHOLE = [("W", 1, 0), ("W", 3, 0), ("W", 0, 1), ("W", 0, 3), ("W", 2, 0), ("W", 0, 2)]
HALVES = [(part, a, b) for part in "AB" for a in (1, 2, 3) for b in (1, 2, 3)]
OWN = ("W", 0, 0)
ITEM = {key: n for n, key in enumerate(WHOLE + HALVES)}


def copy_rows(part, depth):
    return depth if part == "W" else depth // 2


class Gather:
    def __init__(self, number, shard, full, sends, receives, pair_sends, pair_receives, place):
        self.number, self.shard, self.full = number, shard, full
        self.sems = (sends, receives, pair_sends, pair_receives)
        self.place = place
        self.depth = shard.shape[0]
        self.sent = 0

    def slot(self, a, b, other=False):
        x, y, core, turn = self.place
        if other:
            core, turn = 1 - core, -turn
        across = lax.rem(x + turn * a + 2 * SIDE, SIDE)
        along = lax.rem(y + turn * b + 2 * SIDE, SIDE)
        return (along * SIDE + across) * 2 + core

    def rows(self, key, other=False):
        part, a, b = key
        first = self.slot(a, b, other) * self.depth
        count = copy_rows(part, self.depth)
        if part == "B":
            first = first + count
        return self.full.at[pl.ds(pl.multiple_of(first, count), count)]

    def copy(self, key, received, target):
        sends, receives = self.sems[:2]
        n = ITEM[received]
        view = self.rows(key)
        return pltpu.make_async_remote_copy(
            src_ref=self.shard if key == OWN else view,
            dst_ref=view,
            send_sem=sends.at[self.number],
            recv_sem=receives.at[self.number, n],
            device_id={"dp": target},
            device_id_type=MESH,
        )

    def send(self, key, dx, dy):
        part, a, b = key
        received = (part, (a - dx) % SIDE, (b - dy) % SIDE)
        copy = self.copy(key, received, self.slot(dx, dy))
        copy.start()
        self.sent += copy_rows(part, self.depth)

    def wait(self, key):
        self.copy(key, key, self.slot(1, 0)).wait_recv()

    def pair_copy(self, a, b, other=False):
        x, y, core, turn = self.place
        view = self.rows(("W", a, b), other)
        return pltpu.make_async_remote_copy(
            src_ref=view if a or b or other else self.shard,
            dst_ref=view,
            send_sem=self.sems[2].at[self.number],
            recv_sem=self.sems[3].at[self.number],
            device_id={"dp": (y * SIDE + x) * 2 + 1 - core},
            device_id_type=MESH,
        )

    def share(self, a, b):
        self.pair_copy(a, b).start()

    def begin(self):
        for dx, dy in ((1, 0), (0, 1), (-1, 0), (0, -1)):
            self.send(OWN, dx, dy)
        self.share(0, 0)
        self.rows(OWN)[...] = self.shard[...]

    def first(self):
        for a in (3, 1):
            self.wait(("W", a, 0))
            if a == 3:
                self.send(("W", 3, 0), 1, 0)
            for dy in (1, -1):
                self.send(("A", a, 0), 0, dy)
            self.wait(("W", 0, a))
            if a == 3:
                self.send(("W", 0, 3), 0, 1)
            for dx in (1, -1):
                self.send(("B", 0, a), dx, 0)
            self.share(a, 0)
            self.share(0, a)

    def second(self):
        for a in (3, 1):
            self.wait(("A", a, 3))
            self.send(("A", a, 3), 0, 1)
            self.wait(("B", 3, a))
            self.send(("B", 3, a), 1, 0)
        self.wait(("W", 2, 0))
        for dy in (1, -1):
            self.send(("A", 2, 0), 0, dy)
        self.wait(("W", 0, 2))
        for dx in (1, -1):
            self.send(("B", 0, 2), dx, 0)
        self.share(2, 0)
        self.share(0, 2)
        for a in (3, 1):
            self.wait(("A", a, 1))
            self.wait(("B", 1, a))
        for a in (3, 1):
            for b in (3, 1):
                self.share(a, b)

    def third(self):
        self.wait(("A", 2, 3))
        self.send(("A", 2, 3), 0, 1)
        self.wait(("B", 3, 2))
        self.send(("B", 3, 2), 1, 0)
        for a in (3, 1):
            self.wait(("A", a, 2))
            self.wait(("B", 2, a))
        self.wait(("A", 2, 1))
        self.wait(("B", 1, 2))
        for a in (3, 1):
            self.share(2, a)
            self.share(a, 2)

    def fourth(self):
        self.wait(("A", 2, 2))
        self.wait(("B", 2, 2))
        self.share(2, 2)

    def bulk(self, rows, send_sem, receive_sem):
        view = self.full.at[pl.ds(0, rows)]
        return pltpu.make_async_remote_copy(
            src_ref=view,
            dst_ref=view,
            send_sem=send_sem.at[self.number],
            recv_sem=receive_sem.at[self.number],
            device_id={"dp": self.slot(1, 0)},
            device_id_type=MESH,
        )

    def complete(self):
        self.bulk(SIDE * SIDE * self.depth, self.sems[2], self.sems[3]).wait_recv()

    def drain(self):
        self.bulk(self.sent, self.sems[0], self.sems[3]).wait_send()
        self.bulk(SIDE * SIDE * self.depth, self.sems[2], self.sems[3]).wait_send()


def kernel(
    tokens, query_shard, key_shard, value_shard, forget_weight, forget_bias, out,
    near, query_all, key_all, value_all, keys, values, gates, key_extra, queries, totals, peaks, sums,
    sends, receives, pair_sends, pair_receives, ring_sends, ring_receives, near_sends, near_receives,
):
    ring = lax.axis_size("sp")
    half = ring // 2
    me = lax.axis_index("sp")
    mine = lax.axis_index("dp")
    core = lax.rem(mine, 2)
    x = lax.rem(lax.div(mine, 2), SIDE)
    y = lax.div(mine, 2 * SIDE)
    place = (x, y, core, 1 - 2 * core)
    rows = tokens.shape[0]
    heads = forget_weight.shape[0]
    groups, dim = keys.shape[1], keys.shape[3]
    share = heads // groups
    root = math.sqrt(dim)

    gather_keys, gather_values, gather_queries = (
        Gather(n, shard, full, sends, receives, pair_sends, pair_receives, place)
        for n, (shard, full) in enumerate(
            ((key_shard, key_all), (value_shard, value_all), (query_shard, query_all))
        )
    )

    above, below = lax.rem(me + 1, ring), lax.rem(me + ring - 1, ring)
    barrier = pltpu.get_barrier_semaphore()
    for dx, dy in ((1, 0), (0, 1), (-1, 0), (0, -1)):
        pl.semaphore_signal(
            barrier, inc=1, device_id={"dp": gather_keys.slot(dx, dy)}, device_id_type=MESH
        )
    pl.semaphore_signal(barrier, inc=1, device_id={"dp": mine + 1 - 2 * core}, device_id_type=MESH)
    for neighbour in (above, below):
        pl.semaphore_signal(barrier, inc=1, device_id={"sp": neighbour}, device_id_type=MESH)
    pl.semaphore_wait(barrier, 7)

    buffers = {KEYS: keys, VALUES: values, GATES: gates}
    last = {
        (KEYS, UP): half, (KEYS, DOWN): half - 1,
        (VALUES, UP): half - 1, (VALUES, DOWN): half,
        (GATES, UP): half, (GATES, DOWN): half - 1,
    }

    def hop(kind, way, step, slot):
        view = buffers[kind].at[slot]
        return pltpu.make_async_remote_copy(
            src_ref=view,
            dst_ref=view,
            send_sem=ring_sends.at[kind, way, step - 1],
            recv_sem=ring_receives.at[kind, way, step - 1],
            device_id={"sp": above if way == UP else below},
            device_id_type=MESH,
        )

    def origin(way, step):
        return lax.rem(me - step + ring, ring) if way == UP else lax.rem(me + step, ring)

    def launch(kind, way):
        hop(kind, way, 2, origin(way, 1)).start()

    def relay(kind, step):
        for way in (UP, DOWN):
            final = last[kind, way]
            slot = origin(way, step)
            if isinstance(step, int):
                if step <= final:
                    hop(kind, way, step, slot).wait_recv()
                if step < final:
                    hop(kind, way, step + 1, slot).start()
                if 3 <= step <= final:
                    hop(kind, way, step - 1, slot).wait_send()
            else:
                hop(kind, way, step, slot).wait_recv()

                @pl.when(step < final)
                def _():
                    hop(kind, way, step + 1, slot).start()

                hop(kind, way, step - 1, slot).wait_send()

    def visit(way):
        return pltpu.make_async_remote_copy(
            src_ref=tokens,
            dst_ref=near.at[way],
            send_sem=near_sends.at[way],
            recv_sem=near_receives.at[way],
            device_id={"sp": above if way == UP else below},
            device_id_type=MESH,
        )

    wide = gates.shape[2]
    bias_at = lax.broadcasted_iota(jnp.int32, (heads, heads), 0) == lax.broadcasted_iota(jnp.int32, (heads, heads), 1)
    bias = jnp.sum(jnp.where(bias_at, forget_bias[...], 0.0), axis=1, keepdims=True)
    eye = (
        lax.broadcasted_iota(jnp.int32, (rows, wide), 0) == lax.broadcasted_iota(jnp.int32, (rows, wide), 1)
    ).astype(F32).astype(BF16)

    def gate(source, block):
        gate_input = lax.dot_general(forget_weight[...], source[...], NT, preferred_element_type=F32) + bias
        log_gate = (jnp.minimum(gate_input, 0.0) - jnp.log1p(jnp.exp(-jnp.abs(gate_input)))).astype(BF16)
        gates[block] = jnp.dot(log_gate, eye, preferred_element_type=F32).astype(BF16)

    def project(source, weight, buffer, block):
        def one(g, carry):
            columns = pl.ds(pl.multiple_of(g * dim * 2, dim * 2), dim * 2)
            part = jnp.dot(source[...], weight[:, columns], preferred_element_type=F32).astype(BF16)
            buffer[block, 2 * g] = part[:, :dim]
            buffer[block, 2 * g + 1] = part[:, dim:]
            return carry

        lax.fori_loop(0, groups // 2, one, 0)

    lane = lax.broadcasted_iota(jnp.int32, (rows, dim), 1)
    tall = rows + 8
    down = lax.broadcasted_iota(jnp.int32, (tall, wide), 0)
    right = lax.broadcasted_iota(jnp.int32, (tall, wide), 1)
    later = ((right > down) | (down >= rows)).astype(F32).astype(BF16)
    sofar = ((right <= down) & (down < rows)).astype(F32).astype(BF16)

    def thrice(block):
        g = gates[block]
        return jnp.concatenate([g, g, g, jnp.zeros((dim - 3 * heads, wide), BF16)], axis=0)

    def parts(exact):
        hi = exact.astype(BF16).astype(F32)
        rest = exact - hi
        mid = rest.astype(BF16).astype(F32)
        low = rest - mid
        return jnp.where(
            lane < heads, hi, jnp.where(lane < 2 * heads, mid, jnp.where(lane < 3 * heads, low, 0.0))
        )

    ones = ((lane >= 3 * heads) & (lane < 3 * heads + 3)).astype(F32)

    def decay_of(step, after):
        block = lax.rem(me - step + ring, ring)
        summed = lax.dot_general(later, thrice(block), NT, preferred_element_type=F32)
        key_extra[block] = (parts((summed[:rows] + after) * root) + ones).astype(BF16)
        return after + summed[rows : rows + 1]

    def decays():
        own = lax.dot_general(later, thrice(me), NT, preferred_element_type=F32)[rows : rows + 1]
        lax.fori_loop(0, ring, decay_of, -own)

    def query_extras(first, end):
        own_sum = lax.dot_general(sofar, thrice(me), NT, preferred_element_type=F32)[:rows]
        own_parts = parts(own_sum * root).astype(BF16)
        pick_row = lax.broadcasted_iota(jnp.int32, (dim, dim), 0)
        pick_lane = lax.broadcasted_iota(jnp.int32, (dim, dim), 1)

        def query_extra(h, carry):
            pick = ((pick_row == h + heads * (pick_lane - 3 * heads)) & (pick_lane >= 3 * heads)
                    & (pick_lane < 3 * heads + 3)).astype(F32).astype(BF16)
            moved = jnp.dot(own_parts, pick, preferred_element_type=F32)
            hot = ((lane == h) | (lane == h + heads) | (lane == h + 2 * heads)).astype(F32)
            place_rows = pl.ds(pl.multiple_of(lax.rem(h, share) * rows, rows), rows)
            queries[lax.div(h, share), place_rows, dim:] = (moved + hot).astype(BF16)
            return carry

        lax.fori_loop(first, end, query_extra, 0)

    def query_group(g, carry):
        columns = pl.ds(pl.multiple_of(g * dim * share, dim * share), dim * share)
        part = jnp.dot(tokens[...], query_all[:, columns], preferred_element_type=F32).astype(BF16)
        for h in range(share):
            queries[g, h * rows : (h + 1) * rows, :dim] = part[:, h * dim : (h + 1) * dim]
        return carry

    scale = math.log2(math.e) / root
    breadth = share * rows

    def attend(blocks, some_groups, diagonal=False):
        key_rows = rows * len(blocks)
        for g in some_groups:
            key_part = jnp.concatenate(
                [jnp.concatenate([keys[block, g], key_extra[block]], axis=1) for block in blocks], axis=0
            )
            value_part = jnp.concatenate([values[block, g] for block in blocks], axis=0)
            score = lax.dot_general(key_part, queries[g], NT, preferred_element_type=F32)
            if diagonal:
                key_at = lax.broadcasted_iota(jnp.int32, (key_rows, breadth), 0)
                query_at = lax.broadcasted_iota(jnp.int32, (key_rows, breadth), 1)
                for h in range(share - 1, 0, -1):
                    query_at = jnp.where(query_at >= h * rows, query_at - h * rows, query_at)
                score = jnp.where(key_at <= query_at, score, -jnp.inf)
                peak = jnp.max(score, axis=0, keepdims=True)
            else:
                old = peaks[g]
                peak = jnp.maximum(old, jnp.max(score, axis=0, keepdims=True))
            weight = jnp.exp2((score - peak) * scale)
            total = jnp.sum(weight, axis=0, keepdims=True)
            mixed = lax.dot_general(value_part, weight.astype(BF16), TN, preferred_element_type=F32)
            peaks[g] = peak
            if diagonal:
                sums[g] = total
                totals[g] = mixed
            else:
                fade = jnp.exp2((old - peak) * scale)
                sums[g] = sums[g] * fade + total
                totals[g] = totals[g] * fade + mixed

    def attend_own(n, carry):
        attend((me,), (2 * n, 2 * n + 1), diagonal=True)
        return carry

    def unit(u, carry):
        step = lax.div(u, 2) + 1
        some = (2 * lax.rem(u, 2), 2 * lax.rem(u, 2) + 1)
        low, high = me - step, me + step - ring

        @pl.when((low >= 0) & (high >= 0))
        def _():
            attend((low, high), some)

        @pl.when(((low >= 0) | (high >= 0)) & ((low < 0) | (high < 0)))
        def _():
            attend((jnp.maximum(low, high),), some)

        return carry

    gather_keys.begin()
    for way in (UP, DOWN):
        visit(way).start()
    gate(tokens, me)
    gather_keys.first()
    gather_values.begin()
    gather_keys.second()
    gather_values.first()
    gather_keys.third()
    gather_values.second()
    gather_queries.begin()
    gather_keys.fourth()
    gather_keys.complete()
    project(tokens, key_all, keys, me)
    gather_values.third()
    visit(UP).wait_recv()
    gate(near.at[UP], below)
    project(near.at[UP], key_all, keys, below)
    visit(DOWN).wait_recv()
    gate(near.at[DOWN], above)
    launch(GATES, UP)
    launch(KEYS, UP)
    project(near.at[DOWN], key_all, keys, above)
    gather_queries.first()
    launch(GATES, DOWN)
    launch(KEYS, DOWN)
    gather_values.fourth()
    gather_values.complete()
    project(near.at[UP], value_all, values, below)
    project(near.at[DOWN], value_all, values, above)
    relay(GATES, 2)
    launch(VALUES, UP)
    project(tokens, value_all, values, me)
    launch(VALUES, DOWN)
    query_extras(0, heads)
    relay(GATES, 3)
    relay(KEYS, 2)
    gather_queries.second()
    relay(GATES, 4)
    relay(VALUES, 2)
    gather_keys.drain()
    gather_values.drain()
    relay(GATES, 5)
    relay(KEYS, 3)
    gather_queries.third()
    relay(GATES, 6)
    relay(VALUES, 3)
    gather_queries.fourth()
    relay(GATES, 7)
    relay(KEYS, 4)
    for way in (UP, DOWN):
        visit(way).wait_send()
    gather_queries.complete()
    lax.fori_loop(0, groups, query_group, 0)
    relay(GATES, 8)
    relay(VALUES, 4)
    decays()
    lax.fori_loop(0, groups // 2, attend_own, 0)

    def steady(step, carry):
        done = 5 * (step - 5)
        relay(KEYS, step)
        then = jnp.where(step == half - 1, done + 2, done + 3)
        lax.fori_loop(done, then, unit, 0)
        relay(VALUES, step)
        lax.fori_loop(then, jnp.minimum(done + 5, 2 * (half - 1)), unit, 0)
        return carry

    lax.fori_loop(5, half, steady, 0)
    gather_queries.drain()
    relay(KEYS, half)
    relay(VALUES, half)

    @pl.when(me >= half)
    def _():
        attend((me - half,), range(groups))

    for g in range(groups):
        mixed = (totals[g] / sums[g]).T
        for h in range(share):
            at = (g * share + h) * dim
            out[:, at : at + dim] = mixed[h * rows : (h + 1) * rows].astype(BF16)

    for kind in (KEYS, VALUES, GATES):
        for way in (UP, DOWN):
            hop(kind, way, last[kind, way], me).wait_send()


def on_device(tokens, query_weight, key_weight, value_weight, forget_weight, forget_bias):
    token_rows = tokens[0]
    rows, width = token_rows.shape
    ring = lax.axis_size("sp")
    heads = forget_weight.shape[1]
    dim = query_weight.shape[1] // heads
    groups = key_weight.shape[1] // dim
    share = heads // groups
    wide = -(-rows // 128) * 128
    vmem = pl.BlockSpec(memory_space=pltpu.VMEM)
    mixed = pl.pallas_call(
        kernel,
        out_shape=jax.ShapeDtypeStruct((rows, heads * dim), BF16),
        in_specs=[vmem] * 6,
        out_specs=vmem,
        scratch_shapes=[
            pltpu.VMEM((2, rows, width), BF16),
            pltpu.VMEM((width, heads * dim), BF16),
            pltpu.VMEM((width, groups * dim), BF16),
            pltpu.VMEM((width, groups * dim), BF16),
            pltpu.VMEM((ring, groups, rows, dim), BF16),
            pltpu.VMEM((ring, groups, rows, dim), BF16),
            pltpu.VMEM((ring, heads, wide), BF16),
            pltpu.VMEM((ring, rows, dim), BF16),
            pltpu.VMEM((groups, share * rows, 2 * dim), BF16),
            pltpu.VMEM((groups, dim, share * rows), F32),
            pltpu.VMEM((groups, 1, share * rows), F32),
            pltpu.VMEM((groups, 1, share * rows), F32),
            pltpu.SemaphoreType.DMA((3,)),
            pltpu.SemaphoreType.DMA((3, len(ITEM))),
            pltpu.SemaphoreType.DMA((3,)),
            pltpu.SemaphoreType.DMA((3,)),
            pltpu.SemaphoreType.DMA((3, 2, ring // 2)),
            pltpu.SemaphoreType.DMA((3, 2, ring // 2)),
            pltpu.SemaphoreType.DMA((2,)),
            pltpu.SemaphoreType.DMA((2,)),
        ],
        compiler_params=pltpu.CompilerParams(
            collective_id=0, has_side_effects=True, vmem_limit_bytes=32 * 2**20
        ),
    )(token_rows, query_weight, key_weight, value_weight, forget_weight.T, forget_bias[None, :])
    return mixed[None]


def solution(mesh):
    placed = (P("dp", "sp", None), P("dp", None), P("dp", None), P("dp", None), P(), P())
    return jax.shard_map(
        on_device, mesh=mesh, in_specs=placed, out_specs=P("dp", "sp", None), check_vma=False
    )
```

time: 117 us -> 101 us (0.86)
  Pallas kernels: 112 us -> 94.4 us
  local copies, waits for them, and re-layouts: 3.93 us -> 6.14 us
    pallas_call x1, Pallas kernels: 112 us -> 94.4 us  [on_device(): pl.pallas_call(kernel, out_shape=jax.ShapeDtypeStruct((rows, heads * dim)...]
    unnamed x2 -> x13, local copies, waits for them, and re-layouts: 3.93 us -> 6.14 us
where the time goes in v2:
time: 101 us
  Pallas kernels  94.4 us (93%)
  local copies, waits for them, and re-layouts  6.14 us (6%)
    pallas_call x1, Pallas kernels, on_device(): pl.pallas_call(kernel, out_shape=jax.ShapeDtypeStruct((rows, heads * dim)...  94.4 us
    unnamed x13, local copies, waits for them, and re-layouts  6.14 us

profile of v2, /device:TPU:1, one launch (start us, length us, event | category | flops | bytes accessed | tf_op | source)
XLA Modules:
  0.0 100.6 jit_solution(969099756754729643)
XLA Ops:
  0.0 0.0 copy-start.5
  0.0 0.7 copy-done.5
  0.7 0.0 copy-start
  0.7 1.1 %copy-done = bf16[1,192,2048]{2,1,0:T(8,128)(2,1)S(1)} copy-done((bf16[1,192,2048]{2,1,0:T(8,128)(2,1)S(1)}, bf16[1,192,2048]{2,1,0:T(8,128)(2,1)}, u32[]{:S(2)}) %copy-start) | copy-done | bytes 786456
  1.8 0.0 copy-start.1
  1.8 0.9 copy-done.1
  2.7 0.0 copy-start.2
  2.7 0.8 copy-done.2
  3.6 0.0 copy-start.3
  3.6 0.8 copy-done.3
  4.4 0.0 copy-start.4
  4.4 0.8 copy-done.4
  5.3 94.4 %shard_map.64 = bf16[192,2048]{1,0:T(8,128)(2,1)S(1)} custom-call(bf16[192,2048]{1,0:T(8,128)(2,1)S(1)} %bitcast.5, bf16[64,2048]{1,0:T(8,128)(2,1)S(1)} %copy-done.1, bf16[64,512]{1,0:T(8,128)(2,1)S(1)} %copy-done.2, bf16[64,512]{1,0:T(8,128)(2,1)S(1)} %copy-done.3, bf16[16,2048]{1,0:T(8,128)(2,1)S(1)} %bitcast.6, f32[1,16]{1,0:T(1,128)S(1)} %bitcast.7), custom_call_target="tpu_custom_call" | custom-call | tf_op jit(solution)/shard_map/pallas_call | solution.py:491
  99.7 0.9 copy.8
Async XLA Ops:
  0.0 0.7 copy-start.5
  0.7 1.1 %copy-start = (bf16[1,192,2048]{2,1,0:T(8,128)(2,1)S(1)}, bf16[1,192,2048]{2,1,0:T(8,128)(2,1)}, u32[]{:S(2)}) copy-start(bf16[1,192,2048]{2,1,0:T(8,128)(2,1)} %param.6) | copy-start | bytes 2359300
  1.8 0.9 copy-start.1
  2.7 0.8 copy-start.2
  3.6 0.8 copy-start.3
  4.4 0.8 copy-start.4

commit v3 on v2

--- a/solution.py
+++ b/solution.py
@@ -56,7 +56,7 @@
         n = ITEM[received]
         view = self.rows(key)
         return pltpu.make_async_remote_copy(
-            src_ref=self.shard if key == OWN else view,
+            src_ref=view,
             dst_ref=view,
             send_sem=sends.at[self.number],
             recv_sem=receives.at[self.number, n],
@@ -78,7 +78,7 @@
         x, y, core, turn = self.place
         view = self.rows(("W", a, b), other)
         return pltpu.make_async_remote_copy(
-            src_ref=view if a or b or other else self.shard,
+            src_ref=view,
             dst_ref=view,
             send_sem=self.sems[2].at[self.number],
             recv_sem=self.sems[3].at[self.number],
@@ -89,11 +89,15 @@
     def share(self, a, b):
         self.pair_copy(a, b).start()
 
+    def fetch(self, local_sem):
+        self.fetched = pltpu.make_async_copy(self.shard, self.rows(OWN), local_sem)
+        self.fetched.start()
+
     def begin(self):
+        self.fetched.wait()
         for dx, dy in ((1, 0), (0, 1), (-1, 0), (0, -1)):
             self.send(OWN, dx, dy)
         self.share(0, 0)
-        self.rows(OWN)[...] = self.shard[...]
 
     def first(self):
         for a in (3, 1):
@@ -170,9 +174,9 @@
 
 
 def kernel(
-    tokens, query_shard, key_shard, value_shard, forget_weight, forget_bias, out,
-    near, query_all, key_all, value_all, keys, values, gates, key_extra, queries, totals, peaks, sums,
-    sends, receives, pair_sends, pair_receives, ring_sends, ring_receives, near_sends, near_receives,
+    tokens_in, query_shard, key_shard, value_shard, forget_in, bias_in, out,
+    tokens, forget_weight, forget_bias, near, between, chances, query_all, key_all, value_all, keys, values, gates, key_extra, queries, totals, peaks, sums,
+    sends, receives, pair_sends, pair_receives, ring_sends, ring_receives, near_sends, near_receives, local_sems,
 ):
     ring = lax.axis_size("sp")
     half = ring // 2
@@ -188,10 +192,16 @@
     share = heads // groups
     root = math.sqrt(dim)
 
-    gather_keys, gather_values, gather_queries = (
+    part_width = query_all.shape[2]
+    gather_keys, gather_values, gather_left, gather_right = (
         Gather(n, shard, full, sends, receives, pair_sends, pair_receives, place)
         for n, (shard, full) in enumerate(
-            ((key_shard, key_all), (value_shard, value_all), (query_shard, query_all))
+            (
+                (key_shard, key_all),
+                (value_shard, value_all),
+                (query_shard.at[:, pl.ds(0, part_width)], query_all.at[0]),
+                (query_shard.at[:, pl.ds(part_width, part_width)], query_all.at[1]),
+            )
         )
     )
 
@@ -204,17 +214,31 @@
     pl.semaphore_signal(barrier, inc=1, device_id={"dp": mine + 1 - 2 * core}, device_id_type=MESH)
     for neighbour in (above, below):
         pl.semaphore_signal(barrier, inc=1, device_id={"sp": neighbour}, device_id_type=MESH)
+    gather_keys.fetch(local_sems.at[0])
+    fetches = [
+        pltpu.make_async_copy(source, target, local_sems.at[n + 3])
+        for n, (source, target) in enumerate(
+            ((tokens_in, tokens), (forget_in, forget_weight), (bias_in, forget_bias))
+        )
+    ]
+    for fetch in fetches:
+        fetch.start()
+    gather_values.fetch(local_sems.at[1])
+    gather_left.fetch(local_sems.at[2])
+    gather_right.fetch(local_sems.at[6])
     pl.semaphore_wait(barrier, 7)
 
     buffers = {KEYS: keys, VALUES: values, GATES: gates}
     last = {
-        (KEYS, UP): half, (KEYS, DOWN): half - 1,
-        (VALUES, UP): half - 1, (VALUES, DOWN): half,
+        (KEYS, UP): half, (KEYS, DOWN): half,
+        (VALUES, UP): half, (VALUES, DOWN): half,
         (GATES, UP): half, (GATES, DOWN): half - 1,
     }
 
     def hop(kind, way, step, slot):
         view = buffers[kind].at[slot]
+        if kind != GATES and isinstance(step, int) and step == half:
+            view = buffers[kind].at[slot, pl.ds(0, groups - 1) if way == UP else pl.ds(groups - 1, 1)]
         return pltpu.make_async_remote_copy(
             src_ref=view,
             dst_ref=view,
@@ -227,57 +251,133 @@
     def origin(way, step):
         return lax.rem(me - step + ring, ring) if way == UP else lax.rem(me + step, ring)
 
+    def fresh(kind, way, step):
+        if way == UP:
+            return me >= step
+        return (me + step >= ring) | (me + step < last[kind, way])
+
+    def passed(kind, way, step):
+        return (me >= step) & (me < ring - 1) if way == UP else fresh(kind, way, step)
+
     def launch(kind, way):
-        hop(kind, way, 2, origin(way, 1)).start()
+        @pl.when(passed(kind, way, 1))
+        def _():
+            hop(kind, way, 2, origin(way, 1)).start()
+
+    def first_hop(way, part, slot):
+        view = keys.at[slot, :, pl.ds(part * (rows // 2), rows // 2)]
+        return pltpu.make_async_remote_copy(
+            src_ref=view,
+            dst_ref=view,
+            send_sem=ring_sends.at[KEYS, way, part],
+            recv_sem=ring_receives.at[KEYS, way, part],
+            device_id={"sp": above if way == UP else below},
+            device_id_type=MESH,
+        )
+
+    def launch_keys(way, part):
+        @pl.when(passed(KEYS, way, 1))
+        def _():
+            first_hop(way, part, origin(way, 1)).start()
 
     def relay(kind, step):
         for way in (UP, DOWN):
             final = last[kind, way]
             slot = origin(way, step)
-            if isinstance(step, int):
-                if step <= final:
+            fixed = isinstance(step, int)
+            if fixed and step > final:
+                continue
+
+            @pl.when(fresh(kind, way, step))
+            def _():
+                if fixed and kind == KEYS and step == 2:
+                    first_hop(way, 0, slot).wait_recv()
+                    first_hop(way, 1, slot).wait_recv()
+                else:
                     hop(kind, way, step, slot).wait_recv()
-                if step < final:
-                    hop(kind, way, step + 1, slot).start()
-                if 3 <= step <= final:
-                    hop(kind, way, step - 1, slot).wait_send()
-            else:
-                hop(kind, way, step, slot).wait_recv()
-
-                @pl.when(step < final)
+
+            if not fixed or step < final:
+
+                @pl.when(passed(kind, way, step))
                 def _():
-                    hop(kind, way, step + 1, slot).start()
-
-                hop(kind, way, step - 1, slot).wait_send()
-
-    def visit(way):
+                    if fixed:
+                        hop(kind, way, step + 1, slot).start()
+                    else:
+
+                        @pl.when(step < half - 1)
+                        def _():
+                            hop(kind, way, step + 1, slot).start()
+
+                        @pl.when(step == half - 1)
+                        def _():
+                            hop(kind, way, half, slot).start()
+
+            if not fixed or step >= 3:
+
+                @pl.when(passed(kind, way, step - 2))
+                def _():
+                    if fixed and kind == KEYS and step == 3:
+                        first_hop(way, 0, slot).wait_send()
+                        first_hop(way, 1, slot).wait_send()
+                    else:
+                        hop(kind, way, step - 1, slot).wait_send()
+
+    def visit(way, part):
+        these = pl.ds(part * (rows // 2), rows // 2)
         return pltpu.make_async_remote_copy(
-            src_ref=tokens,
-            dst_ref=near.at[way],
-            send_sem=near_sends.at[way],
-            recv_sem=near_receives.at[way],
+            src_ref=tokens.at[these],
+            dst_ref=near.at[way, these],
+            send_sem=near_sends.at[way, part],
+            recv_sem=near_receives.at[way, part],
             device_id={"sp": above if way == UP else below},
             device_id_type=MESH,
         )
 
+    def visits(act):
+        for part in (0, 1):
+            for way, goes in ((UP, me < ring - 1), (DOWN, me < half)):
+
+                @pl.when(goes)
+                def _():
+                    act(visit(way, part))
+
+    comes = {UP: me >= 1, DOWN: (me == ring - 1) | (me < half - 1)}
+
+    def meet(way, part):
+        @pl.when(comes[way])
+        def _():
+            visit(way, part).wait_recv()
+            project(near.at[way], key_all, keys, origin(way, 1), part * (rows // 2), rows // 2)
+
+    def meet_gates(way):
+        @pl.when(comes[way])
+        def _():
+            gate(near.at[way], origin(way, 1))
+
+    def meet_values(way):
+        @pl.when(comes[way])
+        def _():
+            project(near.at[way], value_all, values, origin(way, 1))
+
     wide = gates.shape[2]
-    bias_at = lax.broadcasted_iota(jnp.int32, (heads, heads), 0) == lax.broadcasted_iota(jnp.int32, (heads, heads), 1)
-    bias = jnp.sum(jnp.where(bias_at, forget_bias[...], 0.0), axis=1, keepdims=True)
     eye = (
         lax.broadcasted_iota(jnp.int32, (rows, wide), 0) == lax.broadcasted_iota(jnp.int32, (rows, wide), 1)
     ).astype(F32).astype(BF16)
 
     def gate(source, block):
+        bias_at = lax.broadcasted_iota(jnp.int32, (heads, heads), 0) == lax.broadcasted_iota(jnp.int32, (heads, heads), 1)
+        bias = jnp.sum(jnp.where(bias_at, forget_bias[...], 0.0), axis=1, keepdims=True)
         gate_input = lax.dot_general(forget_weight[...], source[...], NT, preferred_element_type=F32) + bias
         log_gate = (jnp.minimum(gate_input, 0.0) - jnp.log1p(jnp.exp(-jnp.abs(gate_input)))).astype(BF16)
         gates[block] = jnp.dot(log_gate, eye, preferred_element_type=F32).astype(BF16)
 
-    def project(source, weight, buffer, block):
+    def project(source, weight, buffer, block, first=0, count=rows):
         def one(g, carry):
             columns = pl.ds(pl.multiple_of(g * dim * 2, dim * 2), dim * 2)
-            part = jnp.dot(source[...], weight[:, columns], preferred_element_type=F32).astype(BF16)
-            buffer[block, 2 * g] = part[:, :dim]
-            buffer[block, 2 * g + 1] = part[:, dim:]
+            these = source[pl.ds(first, count), :]
+            part = jnp.dot(these, weight[:, columns], preferred_element_type=F32).astype(BF16)
+            buffer[block, 2 * g, pl.ds(first, count)] = part[:, :dim]
+            buffer[block, 2 * g + 1, pl.ds(first, count)] = part[:, dim:]
             return carry
 
         lax.fori_loop(0, groups // 2, one, 0)
@@ -304,15 +404,20 @@
 
     ones = ((lane >= 3 * heads) & (lane < 3 * heads + 3)).astype(F32)
 
-    def decay_of(step, after):
-        block = lax.rem(me - step + ring, ring)
-        summed = lax.dot_general(later, thrice(block), NT, preferred_element_type=F32)
-        key_extra[block] = (parts((summed[:rows] + after) * root) + ones).astype(BF16)
-        return after + summed[rows : rows + 1]
-
-    def decays():
-        own = lax.dot_general(later, thrice(me), NT, preferred_element_type=F32)[rows : rows + 1]
-        lax.fori_loop(0, ring, decay_of, -own)
+    def decay_of(step, carry):
+        @pl.when(me >= step)
+        def _():
+            block = lax.rem(me - step + ring, ring)
+            summed = lax.dot_general(later, thrice(block), NT, preferred_element_type=F32)
+            after = between[...]
+            key_extra[block] = (parts((summed[:rows] + after) * root) + ones).astype(BF16)
+            between[...] = after + summed[rows : rows + 1]
+
+        return carry
+
+    def decay_own():
+        between[...] = -lax.dot_general(later, thrice(me), NT, preferred_element_type=F32)[rows : rows + 1]
+        decay_of(0, 0)
 
     def query_extras(first, end):
         own_sum = lax.dot_general(sofar, thrice(me), NT, preferred_element_type=F32)[:rows]
@@ -332,8 +437,9 @@
         lax.fori_loop(first, end, query_extra, 0)
 
     def query_group(g, carry):
-        columns = pl.ds(pl.multiple_of(g * dim * share, dim * share), dim * share)
-        part = jnp.dot(tokens[...], query_all[:, columns], preferred_element_type=F32).astype(BF16)
+        at = pl.multiple_of(lax.rem(g, groups // 2) * dim * share, dim * share)
+        weight = query_all[lax.div(g, groups // 2), :, pl.ds(at, dim * share)]
+        part = jnp.dot(tokens[...], weight, preferred_element_type=F32).astype(BF16)
         for h in range(share):
             queries[g, h * rows : (h + 1) * rows, :dim] = part[:, h * dim : (h + 1) * dim]
         return carry
@@ -376,96 +482,133 @@
         return carry
 
     def unit(u, carry):
-        step = lax.div(u, 2) + 1
+        pair = lax.div(u, 2)
         some = (2 * lax.rem(u, 2), 2 * lax.rem(u, 2) + 1)
-        low, high = me - step, me + step - ring
-
-        @pl.when((low >= 0) & (high >= 0))
-        def _():
-            attend((low, high), some)
-
-        @pl.when(((low >= 0) | (high >= 0)) & ((low < 0) | (high < 0)))
-        def _():
-            attend((jnp.maximum(low, high),), some)
+        over = (pair == 2) | (pair == 3) | (pair == 5)
+        step = jnp.where(pair < 2, 2 * pair + 1, jnp.where(pair < 4, 2 * pair - 3, jnp.where(pair < 6, 5, 7)))
+        one = jnp.where(over, me + step - ring, me - step)
+        two = jnp.where(pair == 6, me + step - ring, jnp.where(over, me + step + 1 - ring, me - step - 1))
+
+        @pl.when((one >= 0) & (two >= 0))
+        def _():
+            attend((one, two), some)
+
+        @pl.when(((one >= 0) | (two >= 0)) & ((one < 0) | (two < 0)))
+        def _():
+            attend((jnp.maximum(one, two),), some)
 
         return carry
 
     gather_keys.begin()
-    for way in (UP, DOWN):
-        visit(way).start()
+    for fetch in fetches:
+        fetch.wait()
+    visits(lambda copy: copy.start())
     gate(tokens, me)
     gather_keys.first()
     gather_values.begin()
+    decay_own()
     gather_keys.second()
     gather_values.first()
     gather_keys.third()
     gather_values.second()
-    gather_queries.begin()
     gather_keys.fourth()
     gather_keys.complete()
-    project(tokens, key_all, keys, me)
+    meet(DOWN, 0)
+    meet(UP, 0)
+    project(tokens, key_all, keys, me, 0, rows // 2)
+    launch_keys(DOWN, 0)
+    launch_keys(UP, 0)
     gather_values.third()
-    visit(UP).wait_recv()
-    gate(near.at[UP], below)
-    project(near.at[UP], key_all, keys, below)
-    visit(DOWN).wait_recv()
-    gate(near.at[DOWN], above)
+    gather_left.begin()
+    gather_right.begin()
+    meet(UP, 1)
+    meet_gates(UP)
     launch(GATES, UP)
-    launch(KEYS, UP)
-    project(near.at[DOWN], key_all, keys, above)
-    gather_queries.first()
+    meet(DOWN, 1)
+    launch_keys(UP, 1)
+    meet_gates(DOWN)
+    launch_keys(DOWN, 1)
+    gather_values.fourth()
     launch(GATES, DOWN)
-    launch(KEYS, DOWN)
-    gather_values.fourth()
     gather_values.complete()
-    project(near.at[UP], value_all, values, below)
-    project(near.at[DOWN], value_all, values, above)
+    meet_values(UP)
+    meet_values(DOWN)
+    launch(VALUES, UP)
+    project(tokens, key_all, keys, me, rows // 2, rows // 2)
+    launch(VALUES, DOWN)
+    gather_left.first()
     relay(GATES, 2)
-    launch(VALUES, UP)
+    relay(KEYS, 2)
+    gather_right.first()
     project(tokens, value_all, values, me)
-    launch(VALUES, DOWN)
     query_extras(0, heads)
     relay(GATES, 3)
-    relay(KEYS, 2)
-    gather_queries.second()
+    relay(VALUES, 2)
+    gather_left.second()
     relay(GATES, 4)
-    relay(VALUES, 2)
+    relay(KEYS, 3)
     gather_keys.drain()
     gather_values.drain()
+    lax.fori_loop(1, 4, decay_of, 0)
+    gather_right.second()
+    lax.fori_loop(4, 5, decay_of, 0)
     relay(GATES, 5)
-    relay(KEYS, 3)
-    gather_queries.third()
+    relay(VALUES, 3)
+    gather_left.third()
+    visits(lambda copy: copy.wait_send())
+    lax.fori_loop(5, 6, decay_of, 0)
     relay(GATES, 6)
-    relay(VALUES, 3)
-    gather_queries.fourth()
+    relay(KEYS, 4)
+    gather_left.fourth()
+    gather_right.third()
+    lax.fori_loop(6, 7, decay_of, 0)
+    gather_right.fourth()
     relay(GATES, 7)
-    relay(KEYS, 4)
-    for way in (UP, DOWN):
-        visit(way).wait_send()
-    gather_queries.complete()
+    relay(VALUES, 4)
+    gather_left.complete()
+    gather_right.complete()
     lax.fori_loop(0, groups, query_group, 0)
+    lax.fori_loop(0, groups // 2, attend_own, 0)
     relay(GATES, 8)
-    relay(VALUES, 4)
-    decays()
-    lax.fori_loop(0, groups // 2, attend_own, 0)
+    relay(KEYS, 5)
+    lax.fori_loop(7, ring, decay_of, 0)
+    lax.fori_loop(0, 2, unit, 0)
+    relay(VALUES, 5)
+    lax.fori_loop(2, 4, unit, 0)
 
     def steady(step, carry):
-        done = 5 * (step - 5)
+        done = 5 * (step - 6) + 4
         relay(KEYS, step)
-        then = jnp.where(step == half - 1, done + 2, done + 3)
-        lax.fori_loop(done, then, unit, 0)
+        lax.fori_loop(done, done + 3, unit, 0)
         relay(VALUES, step)
-        lax.fori_loop(then, jnp.minimum(done + 5, 2 * (half - 1)), unit, 0)
+        lax.fori_loop(done + 3, done + 5, unit, 0)
         return carry
 
-    lax.fori_loop(5, half, steady, 0)
-    gather_queries.drain()
+    lax.fori_loop(6, half, steady, 0)
+    gather_left.drain()
+    gather_right.drain()
     relay(KEYS, half)
-    relay(VALUES, half)
 
     @pl.when(me >= half)
     def _():
-        attend((me - half,), range(groups))
+        block = me - half
+        for g in range(groups):
+            key_part = jnp.concatenate([keys[block, g], key_extra[block]], axis=1)
+            score = lax.dot_general(key_part, queries[g], NT, preferred_element_type=F32)
+            old = peaks[g]
+            peak = jnp.maximum(old, jnp.max(score, axis=0, keepdims=True))
+            weight = jnp.exp2((score - peak) * scale)
+            fade = jnp.exp2((old - peak) * scale)
+            sums[g] = sums[g] * fade + jnp.sum(weight, axis=0, keepdims=True)
+            totals[g] = totals[g] * fade
+            chances[g] = weight.astype(BF16)
+
+    relay(VALUES, half)
+
+    @pl.when(me >= half)
+    def _():
+        for g in range(groups):
+            totals[g] += lax.dot_general(values[me - half, g], chances[g], TN, preferred_element_type=F32)
 
     for g in range(groups):
         mixed = (totals[g] / sums[g]).T
@@ -475,7 +618,10 @@
 
     for kind in (KEYS, VALUES, GATES):
         for way in (UP, DOWN):
-            hop(kind, way, last[kind, way], me).wait_send()
+
+            @pl.when(passed(kind, way, last[kind, way] - 1))
+            def _():
+                hop(kind, way, last[kind, way], me).wait_send()
 
 
 def on_device(tokens, query_weight, key_weight, value_weight, forget_weight, forget_bias):
@@ -488,14 +634,21 @@
     share = heads // groups
     wide = -(-rows // 128) * 128
     vmem = pl.BlockSpec(memory_space=pltpu.VMEM)
+    inputs = (token_rows, query_weight, key_weight, value_weight, forget_weight.T, forget_bias[None, :])
+    inputs = tuple(pltpu.with_memory_space_constraint(a, pltpu.HBM) for a in inputs)
     mixed = pl.pallas_call(
         kernel,
         out_shape=jax.ShapeDtypeStruct((rows, heads * dim), BF16),
-        in_specs=[vmem] * 6,
+        in_specs=[pl.BlockSpec(memory_space=pltpu.HBM)] * 6,
         out_specs=vmem,
         scratch_shapes=[
+            pltpu.VMEM((rows, width), BF16),
+            pltpu.VMEM((heads, width), BF16),
+            pltpu.VMEM((1, heads), F32),
             pltpu.VMEM((2, rows, width), BF16),
-            pltpu.VMEM((width, heads * dim), BF16),
+            pltpu.VMEM((1, dim), F32),
+            pltpu.VMEM((groups, rows, share * rows), BF16),
+            pltpu.VMEM((2, width, heads * dim // 2), BF16),
             pltpu.VMEM((width, groups * dim), BF16),
             pltpu.VMEM((width, groups * dim), BF16),
             pltpu.VMEM((ring, groups, rows, dim), BF16),
@@ -506,19 +659,20 @@
             pltpu.VMEM((groups, dim, share * rows), F32),
             pltpu.VMEM((groups, 1, share * rows), F32),
             pltpu.VMEM((groups, 1, share * rows), F32),
-            pltpu.SemaphoreType.DMA((3,)),
-            pltpu.SemaphoreType.DMA((3, len(ITEM))),
-            pltpu.SemaphoreType.DMA((3,)),
-            pltpu.SemaphoreType.DMA((3,)),
+            pltpu.SemaphoreType.DMA((4,)),
+            pltpu.SemaphoreType.DMA((4, len(ITEM))),
+            pltpu.SemaphoreType.DMA((4,)),
+            pltpu.SemaphoreType.DMA((4,)),
             pltpu.SemaphoreType.DMA((3, 2, ring // 2)),
             pltpu.SemaphoreType.DMA((3, 2, ring // 2)),
-            pltpu.SemaphoreType.DMA((2,)),
-            pltpu.SemaphoreType.DMA((2,)),
+            pltpu.SemaphoreType.DMA((2, 2)),
+            pltpu.SemaphoreType.DMA((2, 2)),
+            pltpu.SemaphoreType.DMA((7,)),
         ],
         compiler_params=pltpu.CompilerParams(
             collective_id=0, has_side_effects=True, vmem_limit_bytes=32 * 2**20
         ),
-    )(token_rows, query_weight, key_weight, value_weight, forget_weight.T, forget_bias[None, :])
+    )(*inputs)
     return mixed[None]
 
 

time: 101 us -> 88.4 us (0.88)
  Pallas kernels: 94.4 us -> 87.4 us
  local copies, waits for them, and re-layouts: 6.14 us -> 0.88 us
    pallas_call x1, Pallas kernels: 94.4 us -> 87.4 us  [on_device(): pl.pallas_call(kernel, out_shape=jax.ShapeDtypeStruct((rows, heads * dim)...]
    unnamed x13 -> x1, local copies, waits for them, and re-layouts: 6.14 us -> 0.88 us
where the time goes in v3:
time: 88.4 us; the launch traced here: 88.3 us
  Pallas kernels  87.4 us (99%)
    pallas_call x1, Pallas kernels, on_device(): pl.pallas_call(kernel, out_shape=jax.ShapeDtypeStruct((rows, heads * dim)...  87.4 us

profile of v3, /device:TPU:1, one launch (start us, length us, event | category | flops | bytes accessed | tf_op | source)
XLA Modules:
  0.0 88.3 jit_solution(11398777156041495764)
XLA Ops:
  0.0 87.4 %shard_map.64 = bf16[192,2048]{1,0:T(8,128)(2,1)S(1)} custom-call(bf16[192,2048]{1,0:T(8,128)(2,1)} %bitcast.5, bf16[64,2048]{1,0:T(8,128)(2,1)} %query_shard.1, bf16[64,512]{1,0:T(8,128)(2,1)} %key_shard.1, bf16[64,512]{1,0:T(8,128)(2,1)} %value_shard.1, bf16[16,2048]{1,0:T(8,128)(2,1)} %bitcast.6, f32[1,16]{1,0:T(1,128)} %bitcast.7), custom_call_target="tpu_custom_call" | custom-call | tf_op jit(solution)/shard_map/pallas_call | solution.py:639
  87.5 0.9 copy.8

commit v4 on v3

--- a/solution.py
+++ b/solution.py
@@ -17,10 +17,18 @@
 NT = (((1,), (1,)), ((), ()))
 TN = (((0,), (0,)), ((), ()))
 
-WHOLE = [("W", 1, 0), ("W", 3, 0), ("W", 0, 1), ("W", 0, 3), ("W", 2, 0), ("W", 0, 2)]
-HALVES = [(part, a, b) for part in "AB" for a in (1, 2, 3) for b in (1, 2, 3)]
+GROUPS = [
+    [("W", 3, 0), ("W", 0, 3)],
+    [("W", 1, 0), ("W", 0, 1)],
+    [("A", 3, 3), ("A", 1, 3), ("B", 3, 3), ("B", 3, 1)],
+    [("W", 2, 0), ("W", 0, 2)],
+    [("A", 3, 1), ("A", 1, 1), ("B", 1, 3), ("B", 1, 1)],
+    [("A", 2, 3), ("B", 3, 2)],
+    [("A", 3, 2), ("A", 1, 2), ("B", 2, 3), ("B", 2, 1), ("A", 2, 1), ("B", 1, 2)],
+    [("A", 2, 2), ("B", 2, 2)],
+]
 OWN = ("W", 0, 0)
-ITEM = {key: n for n, key in enumerate(WHOLE + HALVES)}
+ITEM = {key: n for n, group in enumerate(GROUPS) for key in group}
 
 
 def copy_rows(part, depth):
@@ -71,8 +79,9 @@
         copy.start()
         self.sent += copy_rows(part, self.depth)
 
-    def wait(self, key):
-        self.copy(key, key, self.slot(1, 0)).wait_recv()
+    def wait(self, group):
+        rows = sum(copy_rows(key[0], self.depth) for key in GROUPS[group])
+        self.bulk(rows, self.sems[0].at[self.number], self.sems[1].at[self.number, group]).wait_recv()
 
     def pair_copy(self, a, b, other=False):
         x, y, core, turn = self.place
@@ -100,58 +109,45 @@
         self.share(0, 0)
 
     def first(self):
+        self.wait(0)
+        self.send(("W", 3, 0), 1, 0)
+        self.send(("W", 0, 3), 0, 1)
         for a in (3, 1):
-            self.wait(("W", a, 0))
-            if a == 3:
-                self.send(("W", 3, 0), 1, 0)
-            for dy in (1, -1):
-                self.send(("A", a, 0), 0, dy)
-            self.wait(("W", 0, a))
-            if a == 3:
-                self.send(("W", 0, 3), 0, 1)
-            for dx in (1, -1):
-                self.send(("B", 0, a), dx, 0)
+            if a == 1:
+                self.wait(1)
+            for way in (1, -1):
+                self.send(("A", a, 0), 0, way)
+                self.send(("B", 0, a), way, 0)
             self.share(a, 0)
             self.share(0, a)
 
     def second(self):
+        self.wait(2)
         for a in (3, 1):
-            self.wait(("A", a, 3))
             self.send(("A", a, 3), 0, 1)
-            self.wait(("B", 3, a))
             self.send(("B", 3, a), 1, 0)
-        self.wait(("W", 2, 0))
-        for dy in (1, -1):
-            self.send(("A", 2, 0), 0, dy)
-        self.wait(("W", 0, 2))
-        for dx in (1, -1):
-            self.send(("B", 0, 2), dx, 0)
+        self.wait(3)
+        for way in (1, -1):
+            self.send(("A", 2, 0), 0, way)
+            self.send(("B", 0, 2), way, 0)
         self.share(2, 0)
         self.share(0, 2)
-        for a in (3, 1):
-            self.wait(("A", a, 1))
-            self.wait(("B", 1, a))
+        self.wait(4)
         for a in (3, 1):
             for b in (3, 1):
                 self.share(a, b)
 
     def third(self):
-        self.wait(("A", 2, 3))
+        self.wait(5)
         self.send(("A", 2, 3), 0, 1)
-        self.wait(("B", 3, 2))
         self.send(("B", 3, 2), 1, 0)
-        for a in (3, 1):
-            self.wait(("A", a, 2))
-            self.wait(("B", 2, a))
-        self.wait(("A", 2, 1))
-        self.wait(("B", 1, 2))
+        self.wait(6)
         for a in (3, 1):
             self.share(2, a)
             self.share(a, 2)
 
     def fourth(self):
-        self.wait(("A", 2, 2))
-        self.wait(("B", 2, 2))
+        self.wait(7)
         self.share(2, 2)
 
     def bulk(self, rows, send_sem, receive_sem):
@@ -159,18 +155,20 @@
         return pltpu.make_async_remote_copy(
             src_ref=view,
             dst_ref=view,
-            send_sem=send_sem.at[self.number],
-            recv_sem=receive_sem.at[self.number],
+            send_sem=send_sem,
+            recv_sem=receive_sem,
             device_id={"dp": self.slot(1, 0)},
             device_id_type=MESH,
         )
 
     def complete(self):
-        self.bulk(SIDE * SIDE * self.depth, self.sems[2], self.sems[3]).wait_recv()
+        n = self.number
+        self.bulk(SIDE * SIDE * self.depth, self.sems[2].at[n], self.sems[3].at[n]).wait_recv()
 
     def drain(self):
-        self.bulk(self.sent, self.sems[0], self.sems[3]).wait_send()
-        self.bulk(SIDE * SIDE * self.depth, self.sems[2], self.sems[3]).wait_send()
+        n = self.number
+        self.bulk(self.sent, self.sems[0].at[n], self.sems[3].at[n]).wait_send()
+        self.bulk(SIDE * SIDE * self.depth, self.sems[2].at[n], self.sems[3].at[n]).wait_send()
 
 
 def kernel(
@@ -242,7 +240,7 @@
         return pltpu.make_async_remote_copy(
             src_ref=view,
             dst_ref=view,
-            send_sem=ring_sends.at[kind, way, step - 1],
+            send_sem=ring_sends.at[kind, way, step % 2 if isinstance(step, int) else lax.rem(step, 2)],
             recv_sem=ring_receives.at[kind, way, step - 1],
             device_id={"sp": above if way == UP else below},
             device_id_type=MESH,
@@ -264,21 +262,25 @@
         def _():
             hop(kind, way, 2, origin(way, 1)).start()
 
-    def first_hop(way, part, slot):
-        view = keys.at[slot, :, pl.ds(part * (rows // 2), rows // 2)]
+    def first_hop(kind, way, part, slot):
+        view = (
+            keys.at[slot, :, pl.ds(part * (rows // 2), rows // 2)]
+            if kind == KEYS
+            else values.at[slot, pl.ds(part * (groups // 2), groups // 2)]
+        )
         return pltpu.make_async_remote_copy(
             src_ref=view,
             dst_ref=view,
-            send_sem=ring_sends.at[KEYS, way, part],
-            recv_sem=ring_receives.at[KEYS, way, part],
+            send_sem=ring_sends.at[kind, way, part],
+            recv_sem=ring_receives.at[kind, way, part],
             device_id={"sp": above if way == UP else below},
             device_id_type=MESH,
         )
 
-    def launch_keys(way, part):
-        @pl.when(passed(KEYS, way, 1))
+    def launch_part(kind, way, part):
+        @pl.when(passed(kind, way, 1))
         def _():
-            first_hop(way, part, origin(way, 1)).start()
+            first_hop(kind, way, part, origin(way, 1)).start()
 
     def relay(kind, step):
         for way in (UP, DOWN):
@@ -287,14 +289,28 @@
             fixed = isinstance(step, int)
             if fixed and step > final:
                 continue
+            begins = fixed and step == 2 and kind != GATES
 
             @pl.when(fresh(kind, way, step))
             def _():
-                if fixed and kind == KEYS and step == 2:
-                    first_hop(way, 0, slot).wait_recv()
-                    first_hop(way, 1, slot).wait_recv()
+                if begins:
+                    first_hop(kind, way, 0, slot).wait_recv()
+                    first_hop(kind, way, 1, slot).wait_recv()
                 else:
                     hop(kind, way, step, slot).wait_recv()
+
+            if begins:
+
+                @pl.when(passed(kind, way, 1))
+                def _():
+                    first_hop(kind, way, 0, slot).wait_send()
+                    first_hop(kind, way, 1, slot).wait_send()
+
+            elif not fixed or step > 3 or (step == 3 and kind == GATES):
+
+                @pl.when(passed(kind, way, step - 2))
+                def _():
+                    hop(kind, way, step - 1, slot).wait_send()
 
             if not fixed or step < final:
 
@@ -311,16 +327,6 @@
                         @pl.when(step == half - 1)
                         def _():
                             hop(kind, way, half, slot).start()
-
-            if not fixed or step >= 3:
-
-                @pl.when(passed(kind, way, step - 2))
-                def _():
-                    if fixed and kind == KEYS and step == 3:
-                        first_hop(way, 0, slot).wait_send()
-                        first_hop(way, 1, slot).wait_send()
-                    else:
-                        hop(kind, way, step - 1, slot).wait_send()
 
     def visit(way, part):
         these = pl.ds(part * (rows // 2), rows // 2)
@@ -354,10 +360,10 @@
         def _():
             gate(near.at[way], origin(way, 1))
 
-    def meet_values(way):
+    def meet_values(way, part):
         @pl.when(comes[way])
         def _():
-            project(near.at[way], value_all, values, origin(way, 1))
+            project(near.at[way], value_all, values, origin(way, 1), some=(part, part + 1))
 
     wide = gates.shape[2]
     eye = (
@@ -371,7 +377,7 @@
         log_gate = (jnp.minimum(gate_input, 0.0) - jnp.log1p(jnp.exp(-jnp.abs(gate_input)))).astype(BF16)
         gates[block] = jnp.dot(log_gate, eye, preferred_element_type=F32).astype(BF16)
 
-    def project(source, weight, buffer, block, first=0, count=rows):
+    def project(source, weight, buffer, block, first=0, count=rows, some=(0, groups // 2)):
         def one(g, carry):
             columns = pl.ds(pl.multiple_of(g * dim * 2, dim * 2), dim * 2)
             these = source[pl.ds(first, count), :]
@@ -380,7 +386,7 @@
             buffer[block, 2 * g + 1, pl.ds(first, count)] = part[:, dim:]
             return carry
 
-        lax.fori_loop(0, groups // 2, one, 0)
+        lax.fori_loop(some[0], some[1], one, 0)
 
     lane = lax.broadcasted_iota(jnp.int32, (rows, dim), 1)
     tall = rows + 8
@@ -405,14 +411,11 @@
     ones = ((lane >= 3 * heads) & (lane < 3 * heads + 3)).astype(F32)
 
     def decay_of(step, carry):
-        @pl.when(me >= step)
-        def _():
-            block = lax.rem(me - step + ring, ring)
-            summed = lax.dot_general(later, thrice(block), NT, preferred_element_type=F32)
-            after = between[...]
-            key_extra[block] = (parts((summed[:rows] + after) * root) + ones).astype(BF16)
-            between[...] = after + summed[rows : rows + 1]
-
+        block = lax.rem(me - step + ring, ring)
+        summed = lax.dot_general(later, thrice(block), NT, preferred_element_type=F32)
+        after = between[...]
+        key_extra[block] = (parts((summed[:rows] + after) * root) + ones).astype(BF16)
+        between[...] = after + summed[rows : rows + 1]
         return carry
 
     def decay_own():
@@ -503,47 +506,53 @@
     for fetch in fetches:
         fetch.wait()
     visits(lambda copy: copy.start())
+    gather_values.begin()
     gate(tokens, me)
     gather_keys.first()
-    gather_values.begin()
+    gather_values.first()
     decay_own()
     gather_keys.second()
-    gather_values.first()
+    gather_values.second()
     gather_keys.third()
-    gather_values.second()
+    gather_values.third()
     gather_keys.fourth()
+    gather_left.begin()
+    gather_right.begin()
     gather_keys.complete()
     meet(DOWN, 0)
     meet(UP, 0)
-    project(tokens, key_all, keys, me, 0, rows // 2)
-    launch_keys(DOWN, 0)
-    launch_keys(UP, 0)
-    gather_values.third()
-    gather_left.begin()
-    gather_right.begin()
+    query_extras(0, 1)
+    launch_part(KEYS, DOWN, 0)
+    launch_part(KEYS, UP, 0)
+    gather_values.fourth()
     meet(UP, 1)
     meet_gates(UP)
     launch(GATES, UP)
     meet(DOWN, 1)
-    launch_keys(UP, 1)
+    launch_part(KEYS, UP, 1)
     meet_gates(DOWN)
-    launch_keys(DOWN, 1)
-    gather_values.fourth()
+    launch_part(KEYS, DOWN, 1)
+    gather_values.complete()
     launch(GATES, DOWN)
-    gather_values.complete()
-    meet_values(UP)
-    meet_values(DOWN)
-    launch(VALUES, UP)
-    project(tokens, key_all, keys, me, rows // 2, rows // 2)
-    launch(VALUES, DOWN)
+    meet_values(UP, 0)
+    meet_values(DOWN, 0)
+    query_extras(1, 2)
+    launch_part(VALUES, UP, 0)
+    launch_part(VALUES, DOWN, 0)
+    meet_values(UP, 1)
+    meet_values(DOWN, 1)
+    query_extras(2, 3)
+    launch_part(VALUES, UP, 1)
+    launch_part(VALUES, DOWN, 1)
     gather_left.first()
     relay(GATES, 2)
     relay(KEYS, 2)
     gather_right.first()
-    project(tokens, value_all, values, me)
-    query_extras(0, heads)
+    query_extras(3, heads)
     relay(GATES, 3)
     relay(VALUES, 2)
+    project(tokens, key_all, keys, me)
+    project(tokens, value_all, values, me)
     gather_left.second()
     relay(GATES, 4)
     relay(KEYS, 3)
@@ -562,16 +571,18 @@
     gather_left.fourth()
     gather_right.third()
     lax.fori_loop(6, 7, decay_of, 0)
+    gather_left.complete()
+    lax.fori_loop(0, groups // 2, query_group, 0)
     gather_right.fourth()
+    lax.fori_loop(0, groups // 4, attend_own, 0)
     relay(GATES, 7)
     relay(VALUES, 4)
-    gather_left.complete()
     gather_right.complete()
-    lax.fori_loop(0, groups, query_group, 0)
-    lax.fori_loop(0, groups // 2, attend_own, 0)
+    lax.fori_loop(groups // 2, groups, query_group, 0)
+    lax.fori_loop(groups // 4, groups // 2, attend_own, 0)
     relay(GATES, 8)
     relay(KEYS, 5)
-    lax.fori_loop(7, ring, decay_of, 0)
+    lax.fori_loop(7, ring, decay_of, 0, unroll=3)
     lax.fori_loop(0, 2, unit, 0)
     relay(VALUES, 5)
     lax.fori_loop(2, 4, unit, 0)
@@ -660,10 +671,10 @@
             pltpu.VMEM((groups, 1, share * rows), F32),
             pltpu.VMEM((groups, 1, share * rows), F32),
             pltpu.SemaphoreType.DMA((4,)),
-            pltpu.SemaphoreType.DMA((4, len(ITEM))),
+            pltpu.SemaphoreType.DMA((4, len(GROUPS))),
             pltpu.SemaphoreType.DMA((4,)),
             pltpu.SemaphoreType.DMA((4,)),
-            pltpu.SemaphoreType.DMA((3, 2, ring // 2)),
+            pltpu.SemaphoreType.DMA((3, 2, 2)),
             pltpu.SemaphoreType.DMA((3, 2, ring // 2)),
             pltpu.SemaphoreType.DMA((2, 2)),
             pltpu.SemaphoreType.DMA((2, 2)),

time: 88.4 us -> 86.6 us (0.980)
  Pallas kernels: 87.4 us -> 85.6 us
    pallas_call x1, Pallas kernels: 87.4 us -> 85.6 us  [on_device(): pl.pallas_call(kernel, out_shape=jax.ShapeDtypeStruct((rows, heads * dim)...]
where the time goes in v4:
time: 86.6 us; the launch traced here: 86.5 us
  Pallas kernels  85.6 us (99%)
  local copies, waits for them, and re-layouts  0.88 us (1%)
    pallas_call x1, Pallas kernels, on_device(): pl.pallas_call(kernel, out_shape=jax.ShapeDtypeStruct((rows, heads * dim)...  85.6 us

profile of v4, /device:TPU:1, one launch (start us, length us, event | category | flops | bytes accessed | tf_op | source)
XLA Modules:
  0.0 86.5 jit_solution(12601894327747167447)
XLA Ops:
  0.0 85.6 %shard_map.64 = bf16[192,2048]{1,0:T(8,128)(2,1)S(1)} custom-call(bf16[192,2048]{1,0:T(8,128)(2,1)} %bitcast.5, bf16[64,2048]{1,0:T(8,128)(2,1)} %query_shard.1, bf16[64,512]{1,0:T(8,128)(2,1)} %key_shard.1, bf16[64,512]{1,0:T(8,128)(2,1)} %value_shard.1, bf16[16,2048]{1,0:T(8,128)(2,1)} %bitcast.6, f32[1,16]{1,0:T(1,128)} %bitcast.7), custom_call_target="tpu_custom_call" | custom-call | tf_op jit(solution)/shard_map/pallas_call | solution.py:650
  85.6 0.9 %copy.8 = bf16[1,192,2048]{2,1,0:T(8,128)(2,1)} copy(bf16[1,192,2048]{2,1,0:T(8,128)(2,1)S(1)} %bitcast.4) | data formatting | bytes 1572864

commit v5 on v4

--- a/solution.py
+++ b/solution.py
@@ -235,12 +235,12 @@
 
     def hop(kind, way, step, slot):
         view = buffers[kind].at[slot]
-        if kind != GATES and isinstance(step, int) and step == half:
+        if kind != GATES and step == half:
             view = buffers[kind].at[slot, pl.ds(0, groups - 1) if way == UP else pl.ds(groups - 1, 1)]
         return pltpu.make_async_remote_copy(
             src_ref=view,
             dst_ref=view,
-            send_sem=ring_sends.at[kind, way, step % 2 if isinstance(step, int) else lax.rem(step, 2)],
+            send_sem=ring_sends.at[kind, way, step % 2],
             recv_sem=ring_receives.at[kind, way, step - 1],
             device_id={"sp": above if way == UP else below},
             device_id_type=MESH,
@@ -286,10 +286,9 @@
         for way in (UP, DOWN):
             final = last[kind, way]
             slot = origin(way, step)
-            fixed = isinstance(step, int)
-            if fixed and step > final:
+            if step > final:
                 continue
-            begins = fixed and step == 2 and kind != GATES
+            begins = step == 2 and kind != GATES
 
             @pl.when(fresh(kind, way, step))
             def _():
@@ -306,27 +305,17 @@
                     first_hop(kind, way, 0, slot).wait_send()
                     first_hop(kind, way, 1, slot).wait_send()
 
-            elif not fixed or step > 3 or (step == 3 and kind == GATES):
+            elif step > 3 or (step == 3 and kind == GATES):
 
                 @pl.when(passed(kind, way, step - 2))
                 def _():
                     hop(kind, way, step - 1, slot).wait_send()
 
-            if not fixed or step < final:
+            if step < final:
 
                 @pl.when(passed(kind, way, step))
                 def _():
-                    if fixed:
-                        hop(kind, way, step + 1, slot).start()
-                    else:
-
-                        @pl.when(step < half - 1)
-                        def _():
-                            hop(kind, way, step + 1, slot).start()
-
-                        @pl.when(step == half - 1)
-                        def _():
-                            hop(kind, way, half, slot).start()
+                    hop(kind, way, step + 1, slot).start()
 
     def visit(way, part):
         these = pl.ds(part * (rows // 2), rows // 2)
@@ -585,17 +574,28 @@
     lax.fori_loop(7, ring, decay_of, 0, unroll=3)
     lax.fori_loop(0, 2, unit, 0)
     relay(VALUES, 5)
-    lax.fori_loop(2, 4, unit, 0)
-
-    def steady(step, carry):
-        done = 5 * (step - 6) + 4
+    lax.fori_loop(2, 5, unit, 0)
+
+    def finish():
+        for g in range(groups):
+            mixed = (totals[g] / sums[g]).T
+            for h in range(share):
+                at = (g * share + h) * dim
+                out[:, at : at + dim] = mixed[h * rows : (h + 1) * rows].astype(BF16)
+
+    for step in (6, half - 1):
+        done = 5 * (step - 6) + 5
         relay(KEYS, step)
-        lax.fori_loop(done, done + 3, unit, 0)
+        lax.fori_loop(done, done + 2, unit, 0)
+        if step == half - 1:
+
+            @pl.when(me < half - 1)
+            def _():
+                finish()
+
         relay(VALUES, step)
-        lax.fori_loop(done + 3, done + 5, unit, 0)
-        return carry
-
-    lax.fori_loop(6, half, steady, 0)
+        lax.fori_loop(done + 2, min(done + 5, 2 * (half - 1)), unit, 0)
+
     gather_left.drain()
     gather_right.drain()
     relay(KEYS, half)
@@ -621,11 +621,9 @@
         for g in range(groups):
             totals[g] += lax.dot_general(values[me - half, g], chances[g], TN, preferred_element_type=F32)
 
-    for g in range(groups):
-        mixed = (totals[g] / sums[g]).T
-        for h in range(share):
-            at = (g * share + h) * dim
-            out[:, at : at + dim] = mixed[h * rows : (h + 1) * rows].astype(BF16)
+    @pl.when(me >= half - 1)
+    def _():
+        finish()
 
     for kind in (KEYS, VALUES, GATES):
         for way in (UP, DOWN):

time: 86.6 us -> 86.6 us (level)
  no operation moved by 1% of the time
where the time goes in v5:
time: 86.6 us; the launch traced here: 86.5 us
  Pallas kernels  85.6 us (99%)
  local copies, waits for them, and re-layouts  0.88 us (1%)
    pallas_call x1, Pallas kernels, on_device(): pl.pallas_call(kernel, out_shape=jax.ShapeDtypeStruct((rows, heads * dim)...  85.6 us

profile of v5, /device:TPU:1, one launch (start us, length us, event | category | flops | bytes accessed | tf_op | source)
XLA Modules:
  0.0 86.5 jit_solution(1442194073188936500)
XLA Ops:
  0.0 85.6 %shard_map.64 = bf16[192,2048]{1,0:T(8,128)(2,1)S(1)} custom-call(bf16[192,2048]{1,0:T(8,128)(2,1)} %bitcast.5, bf16[64,2048]{1,0:T(8,128)(2,1)} %query_shard.1, bf16[64,512]{1,0:T(8,128)(2,1)} %key_shard.1, bf16[64,512]{1,0:T(8,128)(2,1)} %value_shard.1, bf16[16,2048]{1,0:T(8,128)(2,1)} %bitcast.6, f32[1,16]{1,0:T(1,128)} %bitcast.7), custom_call_target="tpu_custom_call" | custom-call | tf_op jit(solution)/shard_map/pallas_call | solution.py:648
  85.6 0.9 %copy.8 = bf16[1,192,2048]{2,1,0:T(8,128)(2,1)} copy(bf16[1,192,2048]{2,1,0:T(8,128)(2,1)S(1)} %bitcast.4) | data formatting | bytes 1572864
